TPU v7x, 128 devices: a whole 4x4x4 slice. The times are simulated.
128 devices in a mesh: sp: 16 (over z, x), tp: 8 (over y, core).
Axes of the slice: x: 4, y: 4, z: 4, core: 2. Of those that a mesh axis runs over, the one named last changes fastest.
Arguments:
- tokens: bfloat16 [2048, 1024], P('sp', 'tp'), may hold values from -6 to 6
- norm_gain: float32 [3, 1024], replicated, may hold values from 0.1 to 1.9
- w_query: bfloat16 [3, 1024, 1024], P(None, 'sp', 'tp'), may hold values from -0.1875 to 0.1875
- w_key: bfloat16 [3, 1024, 1024], P(None, 'sp', 'tp'), may hold values from -0.1875 to 0.1875
- w_value: bfloat16 [3, 1024, 1024], P(None, 'sp', 'tp'), may hold values from -0.1875 to 0.1875
- w_out: bfloat16 [3, 1024, 1024], P(None, 'tp', 'sp'), may hold values from -0.5625 to 0.5625
- offset_bias: float32 [3, 16, 8, 16], P(None, 'tp'), may hold values from -3 to 3
- documents: int32 [2048], P('sp'), may hold values from 0 to 15, never falling along the last dimension, each value on 1 to 256 neighbouring positions
Outputs:
- mixed: bfloat16 [2048, 1024], P('sp', 'tp')
Inputs may be any that keep to these rules, and one draw needn't show every extreme that they name: `documents`: document numbers never fall along the token order, start at 0, and each document has 1 to 256 tokens.
All inputs are finite; a program needn't handle non-finite values.
Results may differ from a plain program's by a relative error of at most 0.02.
Values may be sent and summed in bfloat16 or wider, within the bound.
A program may use at most 64 MiB of HBM per device.

v0:
```python
import jax
import jax.numpy as jnp
from jax import lax
from jax.sharding import Mesh
from jax.sharding import PartitionSpec as P

HEAD_DIM = 64
WIN_ROWS = 8
WIN_COLS = 16
LAYERS = 3
GRID_W = 32
TP = ("tp_0", "tp_1")


EPS = 1e-06


def with_halo(shard, sides, width, wrap):
    for axis, dim in sides:
        count, length = lax.axis_size(axis), shard.shape[dim]
        up = [(i, (i + 1) % count) for i in range(count if wrap else count - 1)]
        down = [(j, i) for i, j in up]
        last = lax.slice_in_dim(shard, length - width, length, axis=dim)
        leading = lax.slice_in_dim(shard, 0, width, axis=dim)
        before = lax.ppermute(last, axis, up)
        after = lax.ppermute(leading, axis, down)
        shard = jnp.concatenate([before, shard, after], axis=dim)
    return shard


def laid_out(blocks, dim):
    dims = list(blocks.shape[1:])
    dims[dim] *= blocks.shape[0]
    return jnp.moveaxis(blocks, 0, dim).reshape(dims)


def gather_together(arrays, axis, dims):
    ravelled = jnp.concatenate([a.reshape(-1) for a in arrays])
    lines, at, done = lax.all_gather(ravelled, axis), 0, []
    for a, dim in zip(arrays, dims):
        blocks = lines[:, at : at + a.size].reshape(-1, *a.shape)
        done.append(laid_out(blocks, dim))
        at += a.size
    return tuple(done)


def stacked_from(shard, axes, sequence):
    blocks = shard[None]
    for k in sequence:
        blocks = lax.all_gather(blocks, axes[k], axis=0, tiled=True)
    current = [lax.axis_size(axes[k]) for k in reversed(sequence)]
    blocks = blocks.reshape(*current, *shard.shape)
    turned = sorted(range(len(sequence)), key=lambda place: sequence[len(sequence) - 1 - place])
    return blocks.transpose(*turned, *range(len(sequence), blocks.ndim)).reshape(-1, *shard.shape)


def whole_of(shard, axes, sequence, dim):
    return laid_out(stacked_from(shard, axes, sequence), dim)


def rms_rows(stream, gain_row):
    values = stream.astype(jnp.float32)
    mean_sq = jnp.mean(values * values, axis=-1, keepdims=True)
    return (values * lax.rsqrt(mean_sq + EPS) * gain_row).astype(jnp.bfloat16)


def head_norm(heads_raw):
    values = heads_raw.astype(jnp.float32)
    mean_sq = jnp.mean(values * values, axis=-1, keepdims=True)
    return (values * lax.rsqrt(mean_sq + EPS)).astype(jnp.bfloat16)


def attend(queries, fringe, seg_own, seg_fringe, bias_layer):
    row_count, grid_width, head_count, head_width = queries.shape
    key_rows = jnp.stack(
        [fringe[row_lag : row_lag + row_count] for row_lag in range(WIN_ROWS)], axis=1
    )
    seg_rows = jnp.stack(
        [seg_fringe[row_lag : row_lag + row_count] for row_lag in range(WIN_ROWS)], axis=1
    )
    key_part = key_rows[..., :head_width]
    value_part = key_rows[..., head_width:]
    scores = jnp.einsum(
        "rchd,rjkhd->rhcjk", queries, key_part, preferred_element_type=jnp.float32
    ) * head_width ** (-0.5)
    column = jnp.arange(grid_width)
    col_offset = column[None, :] - column[:, None] + WIN_COLS // 2
    inside = (col_offset >= 0) & (col_offset < WIN_COLS)
    bias_table = bias_layer[:, :, jnp.clip(col_offset, 0, WIN_COLS - 1)]
    scores = scores + jnp.transpose(bias_table, (0, 2, 1, 3))[None]
    same_doc = seg_rows[:, None, None, :, :] == seg_own[:, None, :, None, None]
    allowed = same_doc & inside[None, None, :, None, :]
    scores = jnp.where(allowed, scores, -1e30)
    flat = scores.reshape(row_count, head_count, grid_width, WIN_ROWS * grid_width)
    attn_probs = jax.nn.softmax(flat, axis=-1).astype(jnp.bfloat16)
    attn_probs = attn_probs.reshape(row_count, head_count, grid_width, WIN_ROWS, grid_width)
    mixed_heads = jnp.einsum(
        "rhcjk,rjkhd->rchd", attn_probs, value_part, preferred_element_type=jnp.float32
    )
    return mixed_heads.astype(jnp.bfloat16)


def local(tokens, norm_gain, w_query, w_key, w_value, w_out, offset_bias, documents):
    token_count = tokens.shape[0]
    row_count = token_count // GRID_W
    reach_rows = WIN_ROWS // 2
    head_count = offset_bias.shape[1]
    seg_own = (documents + 1).reshape(row_count, GRID_W)
    seg_fringe = with_halo(seg_own, (("sp", 0),), reach_rows, False)
    collected = gather_together((w_query, w_key, w_value, w_out), "sp", (1, 1, 1, 2))
    stream = tokens
    for layer_index in range(LAYERS):
        gathered = whole_of(stream, ("tp_0", "tp_1"), (0, 1), 1)
        normed = rms_rows(gathered, norm_gain[layer_index])
        query_raw = jnp.dot(normed, collected[0][layer_index], preferred_element_type=jnp.float32)
        key_raw = jnp.dot(normed, collected[1][layer_index], preferred_element_type=jnp.float32)
        value_raw = jnp.dot(normed, collected[2][layer_index], preferred_element_type=jnp.float32)
        query_heads = head_norm(
            query_raw.astype(jnp.bfloat16).reshape(row_count, GRID_W, head_count, HEAD_DIM)
        )
        key_heads = head_norm(
            key_raw.astype(jnp.bfloat16).reshape(row_count, GRID_W, head_count, HEAD_DIM)
        )
        value_heads = value_raw.astype(jnp.bfloat16).reshape(
            row_count, GRID_W, head_count, HEAD_DIM
        )
        key_value = jnp.concatenate([key_heads, value_heads], axis=-1)
        fringe = with_halo(key_value, (("sp", 0),), reach_rows, False)
        attended = attend(query_heads, fringe, seg_own, seg_fringe, offset_bias[layer_index])
        attended = attended.reshape(token_count, head_count * HEAD_DIM)
        partial_sums = jnp.dot(
            attended, collected[3][layer_index], preferred_element_type=jnp.float32
        )
        stream = (
            lax.psum_scatter(partial_sums.astype(jnp.bfloat16), TP, scatter_dimension=1, tiled=True)
            .astype(jnp.float32)
            .astype(jnp.bfloat16)
        )
    return stream


def solution(mesh):
    torus = Mesh(mesh.devices.reshape(mesh.shape["sp"], 4, 2), ("sp", "tp_0", "tp_1"))
    return jax.shard_map(
        local,
        mesh=torus,
        in_specs=(
            P("sp", TP),
            P(),
            P(None, "sp", TP),
            P(None, "sp", TP),
            P(None, "sp", TP),
            P(None, TP, "sp"),
            P(None, TP, None, None),
            P("sp"),
        ),
        out_specs=P("sp", TP),
        check_vma=False,
    )
```

profile of v0, /device:TPU:1, one launch (start us, length us, event | category | flops | bytes accessed | tf_op | source)
XLA Modules:
  0.0 246.8 jit_solution(3143307342069625789)
XLA Ops:
  6.5 0.9 copy.207
  7.6 1.6 pad_maximum_fusion
  9.2 0.7 broadcast_add_fusion
  10.0 3.9 %collective-permute-start.2 = (s32[4,32]{1,0:T(4,128)S(1)}, s32[4,32]{1,0:T(4,128)S(1)}, u32[]{:S(2)}, u32[]{:S(2)}) collective-permute-start(s32[4,32]{1,0:T(4,128)S(1)} %reshape.364), channel_id=1, source_target_pairs={{0,8},{8,16},{16,24},{24,32},{32,40},{40,48},{48,56},{56,64},{64,7... | collective-permute-start | bytes 1544 | tf_op jit(solution)/shard_map/ppermute | solution.py:25
  13.9 1.3 collective-permute-start.3
  15.2 10.3 %all-gather = bf16[512,128]{1,0:T(8,128)(2,1)S(1)} all-gather(bf16[128,128]{1,0:T(8,128)(2,1)} %param.8), channel_id=2, replica_groups=mesh['sp'=16,'tp_0'=4,'tp_1'=2] {'tp_0'}, dimensions={0}, use_global_device_ids=true | all-gather | bytes 163840 | tf_op jit(solution)/shard_map/all_gather | solution.py:50
  25.5 5.0 %all_gather.25 = bf16[8,128,128]{2,1,0:T(8,128)(2,1)S(1)} all-gather(bf16[4,128,128]{2,1,0:T(8,128)(2,1)S(1)} %bitcast.377), channel_id=1, replica_groups=mesh['sp'=16,'tp_0'=4,'tp_1'=2] {'tp_1'}, dimensions={0}, use_global_device_ids=true | all-gather | bytes 393216 | tf_op jit(solution)/shard_map/all_gather | solution.py:50
  32.5 3.5 %gather_fusion = f32[1024,2,8]{2,1,0:T(2,128)S(1)} fusion(f32[2,8,16]{1,0,2:T(2,128)S(1)} %bitcast.325, s32[1024]{0:T(1024)S(1)} %broadcast_clamp_fusion), kind=kCustom, calls=%fused_computation | custom fusion | bytes 135168 | tf_op jit(solution)/shard_map/gather | solution.py:89
  36.1 1.3 copy.224
  37.8 21.3 %all-gather.6.cloned.1.call-done = bf16[1572864]{0:T(1024)(128)(2,1)} async-done(((bf16[98304]{0:T(1024)(128)(2,1)}), bf16[1572864]{0:T(1024)(128)(2,1)}) %all-gather.6.cloned.1.call-update) | async-done | bytes 3145744 | tf_op jit(solution)/shard_map/all_gather | solution.py:39
  59.0 2.8 %reshape.409 = bf16[16,98304]{1,0:T(8,128)(2,1)S(1)} reshape(bf16[1572864]{0:T(1024)(128)(2,1)} %all-gather.6.cloned.1.call-done) | data formatting | bytes 6291456 | tf_op jit(solution)/shard_map/all_gather | solution.py:39
  61.8 1.5 fusion.69
  63.4 0.9 fusion.72
  65.0 0.7 fusion.35
  65.9 0.9 fusion.73
  67.2 1.6 pad_maximum_fusion.4
  68.8 3.7 %collective-permute-start = (bf16[4,32,2,128]{3,1,2,0:T(8,128)(2,1)}, bf16[4,32,2,128]{3,1,2,0:T(8,128)(2,1)}, u32[]{:S(2)}, u32[]{:S(2)}) collective-permute-start(bf16[4,32,2,128]{3,1,2,0:T(8,128)(2,1)} %pad_maximum_fusion.4), channel_id=1, source_target_pairs={{0,8},{8,16},{16,24},{24,32},{32,40},{40,48},{48,56},{56,64},{64,7... | collective-permute-start | bytes 196616 | tf_op jit(solution)/shard_map/ppermute | solution.py:25
  72.5 1.3 collective-permute-start.1
  73.9 0.9 fusion.71
  75.5 1.7 reshape.367
  77.2 0.9 fusion.70
  78.4 1.3 copy.227
  79.6 0.8 constant_dynamic-update-slice_fusion.1
  80.5 1.0 pad_maximum_fusion.1
  81.5 0.9 constant_dynamic-update-slice_fusion
  84.2 0.8 copy.276
  85.2 3.5 %gather_fusion.1 = f32[1024,2,8]{2,1,0:T(2,128)S(1)} fusion(f32[2,8,16]{1,0,2:T(2,128)S(1)} %bitcast.326, s32[1024]{0:T(1024)S(1)} %broadcast_clamp_fusion), kind=kCustom, calls=%fused_computation.1 | custom fusion | bytes 135168 | tf_op jit(solution)/shard_map/gather | solution.py:89
  88.8 0.7 copy.245
  89.7 25.7 %reduce-scatter.10.cloned.1.call-done = bf16[128,128]{1,0:T(8,128)(2,1)} async-done(((bf16[1024,128]{1,0:T(8,128)(2,1)}), bf16[128,128]{1,0:T(8,128)(2,1)}) %reduce-scatter.10.cloned.1.call-update) | async-done | bytes 32784
  115.4 0.9 copy.277
  116.3 10.0 %all-gather.2 = bf16[512,128]{1,0:T(8,128)(2,1)S(1)} all-gather(bf16[128,128]{1,0:T(8,128)(2,1)S(1)} %copy.277), channel_id=4, replica_groups=mesh['sp'=16,'tp_0'=4,'tp_1'=2] {'tp_0'}, dimensions={0}, use_global_device_ids=true | all-gather | bytes 163840 | tf_op jit(solution)/shard_map/all_gather | solution.py:50
  126.3 7.0 %all_gather.29 = bf16[8,128,128]{2,1,0:T(8,128)(2,1)S(1)} all-gather(bf16[4,128,128]{2,1,0:T(8,128)(2,1)S(1)} %bitcast.375), channel_id=1, replica_groups=mesh['sp'=16,'tp_0'=4,'tp_1'=2] {'tp_1'}, dimensions={0}, use_global_device_ids=true | all-gather | bytes 393216 | tf_op jit(solution)/shard_map/all_gather | solution.py:50
  135.2 3.1 %collective-permute-start.4 = (bf16[4,32,2,128]{3,1,2,0:T(8,128)(2,1)S(1)}, bf16[4,32,2,128]{3,1,2,0:T(8,128)(2,1)S(1)}, u32[]{:S(2)}, u32[]{:S(2)}) collective-permute-start(bf16[4,32,2,128]{3,1,2,0:T(8,128)(2,1)S(1)} %pad_maximum_fusion.5), channel_id=1, source_target_pairs={{0,8},{8,16},{16,24},{24,32},{32,40},{40,48},{48,56},{56,64},{64,7... | collective-permute-start | bytes 196616 | tf_op jit(solution)/shard_map/ppermute | solution.py:25
  138.3 1.5 collective-permute-start.5
  140.7 2.6 %collective-permute-done.5 = bf16[4,32,2,128]{3,1,2,0:T(8,128)(2,1)S(1)} collective-permute-done((bf16[4,32,2,128]{3,1,2,0:T(8,128)(2,1)S(1)}, bf16[4,32,2,128]{3,1,2,0:T(8,128)(2,1)S(1)}, u32[]{:S(2)}, u32[]{:S(2)}) %collective-permute-start.5) | collective-permute-done | bytes 65568 | tf_op jit(solution)/shard_map/ppermute | solution.py:26
  145.3 0.9 copy.278
  146.3 3.5 %gather_fusion.2 = f32[1024,2,8]{2,1,0:T(2,128)S(1)} fusion(f32[2,8,16]{1,0,2:T(2,128)S(1)} %bitcast.324, s32[1024]{0:T(1024)S(1)} %broadcast_clamp_fusion), kind=kCustom, calls=%fused_computation.2 | custom fusion | bytes 135168 | tf_op jit(solution)/shard_map/gather | solution.py:89
  149.9 0.7 copy.266
  150.8 26.3 %reduce-scatter.12.cloned.1.call-done = bf16[128,128]{1,0:T(8,128)(2,1)} async-done(((bf16[1024,128]{1,0:T(8,128)(2,1)}), bf16[128,128]{1,0:T(8,128)(2,1)}) %reduce-scatter.12.cloned.1.call-update) | async-done | bytes 32784
  177.1 0.9 copy.279
  178.0 10.0 %all-gather.3 = bf16[512,128]{1,0:T(8,128)(2,1)S(1)} all-gather(bf16[128,128]{1,0:T(8,128)(2,1)S(1)} %copy.279), channel_id=5, replica_groups=mesh['sp'=16,'tp_0'=4,'tp_1'=2] {'tp_0'}, dimensions={0}, use_global_device_ids=true | all-gather | bytes 163840 | tf_op jit(solution)/shard_map/all_gather | solution.py:50
  188.0 7.0 %all_gather.31 = bf16[8,128,128]{2,1,0:T(8,128)(2,1)S(1)} all-gather(bf16[4,128,128]{2,1,0:T(8,128)(2,1)S(1)} %bitcast.376), channel_id=1, replica_groups=mesh['sp'=16,'tp_0'=4,'tp_1'=2] {'tp_1'}, dimensions={0}, use_global_device_ids=true | all-gather | bytes 393216 | tf_op jit(solution)/shard_map/all_gather | solution.py:50
  196.9 3.1 %collective-permute-start.6 = (bf16[4,32,2,128]{3,1,2,0:T(8,128)(2,1)S(1)}, bf16[4,32,2,128]{3,1,2,0:T(8,128)(2,1)S(1)}, u32[]{:S(2)}, u32[]{:S(2)}) collective-permute-start(bf16[4,32,2,128]{3,1,2,0:T(8,128)(2,1)S(1)} %pad_maximum_fusion.6), channel_id=1, source_target_pairs={{0,8},{8,16},{16,24},{24,32},{32,40},{40,48},{48,56},{56,64},{64,7... | collective-permute-start | bytes 196616 | tf_op jit(solution)/shard_map/ppermute | solution.py:25
  200.0 1.3 collective-permute-start.7
  202.2 2.8 %collective-permute-done.7 = bf16[4,32,2,128]{3,1,2,0:T(8,128)(2,1)S(1)} collective-permute-done((bf16[4,32,2,128]{3,1,2,0:T(8,128)(2,1)S(1)}, bf16[4,32,2,128]{3,1,2,0:T(8,128)(2,1)S(1)}, u32[]{:S(2)}, u32[]{:S(2)}) %collective-permute-start.7) | collective-permute-done | bytes 65568 | tf_op jit(solution)/shard_map/ppermute | solution.py:26
  207.0 0.8 copy.280
  207.8 31.0 %reduce-scatter.14.cloned.1.call-done = bf16[128,128]{1,0:T(8,128)(2,1)} async-done(((bf16[1024,128]{1,0:T(8,128)(2,1)}), bf16[128,128]{1,0:T(8,128)(2,1)}) %reduce-scatter.14.cloned.1.call-update) | async-done | bytes 32784
  238.8 1.5 copy.281
  (179 shorter events, 16.5 us)
Async XLA Ops:
  6.5 24.3 %copy-start.16 = (f32[3,1024]{1,0:T(4,128)S(1)}, f32[3,1024]{1,0:T(4,128)}, u32[]{:S(2)}) copy-start(f32[3,1024]{1,0:T(4,128)} %param.9) | copy-start | bytes 36868
  6.5 24.9 %copy-start.14 = (f32[3,2,8,16]{3,2,1,0:T(8,128)S(1)}, f32[3,2,8,16]{3,2,1,0:T(8,128)}, u32[]{:S(2)}) copy-start(f32[3,2,8,16]{3,2,1,0:T(8,128)} %param.14) | copy-start | bytes 9220
  6.5 52.5 %all-gather.6.cloned.1.call-start = ((), (), s32[]{:S(2)}) async-start(), calls=%async_computation.3 | async-start | bytes 3342336 | tf_op jit(solution)/shard_map/all_gather | solution.py:39
  9.2 106.2 %reduce-scatter.10.cloned.1.call-start = ((), (), s32[]{:S(2)}) async-start(), calls=%async_computation.4 | async-start | bytes 294912
  10.0 27.5 %collective-permute-start.2 = (s32[4,32]{1,0:T(4,128)S(1)}, s32[4,32]{1,0:T(4,128)S(1)}, u32[]{:S(2)}, u32[]{:S(2)}) collective-permute-start(s32[4,32]{1,0:T(4,128)S(1)} %reshape.364), channel_id=1, source_target_pairs={{0,8},{8,16},{16,24},{24,32},{32,40},{40,48},{48,56},{56,64},{64,7... | collective-permute-start | bytes 1544 | tf_op jit(solution)/shard_map/ppermute | solution.py:25
  13.9 23.5 %collective-permute-start.3 = (s32[4,32]{1,0:T(4,128)S(1)}, s32[4,32]{1,0:T(4,128)S(1)}, u32[]{:S(2)}, u32[]{:S(2)}) collective-permute-start(s32[4,32]{1,0:T(4,128)S(1)} %reshape.364), channel_id=1, source_target_pairs={{8,0},{16,8},{24,16},{32,24},{40,32},{48,40},{56,48},{64,56},{72,6... | collective-permute-start | bytes 1544 | tf_op jit(solution)/shard_map/ppermute | solution.py:26
  63.3 2.5 %copy-start.1 = (bf16[2,8,192,128]{3,1,2,0:T(8,128)(2,1)S(1)}, bf16[2,8,192,128]{3,1,2,0:T(8,128)(2,1)}, u32[]{:S(2)}) copy-start(bf16[2,8,192,128]{3,1,2,0:T(8,128)(2,1)} %get-tuple-element.7) | copy-start | bytes 2359300
  64.3 9.5 %copy-start = (bf16[2,8,192,128]{3,1,2,0:T(8,128)(2,1)S(1)}, bf16[2,8,192,128]{3,1,2,0:T(8,128)(2,1)}, u32[]{:S(2)}) copy-start(bf16[2,8,192,128]{3,1,2,0:T(8,128)(2,1)} %get-tuple-element.6) | copy-start | bytes 2359300
  65.9 9.5 %copy-start.2 = (bf16[16,24576]{1,0:T(8,128)(2,1)S(1)}, bf16[16,24576]{1,0:T(8,128)(2,1)}, u32[]{:S(2)}) copy-start(bf16[16,24576]{1,0:T(8,128)(2,1)} %get-tuple-element.5) | copy-start | bytes 2359300
  67.2 6.5 %copy-start.11 = (bf16[4,32,2,64]{3,1,2,0:T(8,128)(2,1)}, bf16[4,32,2,64]{3,1,2,0:T(8,128)(2,1)S(1)}, u32[]{:S(2)}) copy-start(bf16[4,32,2,64]{3,1,2,0:T(8,128)(2,1)S(1)} %copy.211) | copy-start | bytes 98308
  68.8 10.8 %collective-permute-start = (bf16[4,32,2,128]{3,1,2,0:T(8,128)(2,1)}, bf16[4,32,2,128]{3,1,2,0:T(8,128)(2,1)}, u32[]{:S(2)}, u32[]{:S(2)}) collective-permute-start(bf16[4,32,2,128]{3,1,2,0:T(8,128)(2,1)} %pad_maximum_fusion.4), channel_id=1, source_target_pairs={{0,8},{8,16},{16,24},{24,32},{32,40},{40,48},{48,56},{56,64},{64,7... | collective-permute-start | bytes 196616 | tf_op jit(solution)/shard_map/ppermute | solution.py:25
  72.5 8.0 %collective-permute-start.1 = (bf16[4,32,2,128]{3,1,2,0:T(8,128)(2,1)}, bf16[4,32,2,128]{3,1,2,0:T(8,128)(2,1)}, u32[]{:S(2)}, u32[]{:S(2)}) collective-permute-start(bf16[4,32,2,128]{3,1,2,0:T(8,128)(2,1)} %pad_maximum_fusion.4), channel_id=1, source_target_pairs={{8,0},{16,8},{24,16},{32,24},{40,32},{48,40},{56,48},{64,56},{72,6... | collective-permute-start | bytes 196616 | tf_op jit(solution)/shard_map/ppermute | solution.py:26
  75.5 5.0 %copy-start.10 = (bf16[4,32,2,64]{3,1,2,0:T(8,128)(2,1)S(1)}, bf16[4,32,2,64]{3,1,2,0:T(8,128)(2,1)}, u32[]{:S(2)}) copy-start(bf16[4,32,2,64]{3,1,2,0:T(8,128)(2,1)} %fusion.35) | copy-start | bytes 98308
  75.5 5.0 %copy-start.12 = (bf16[4,32,2,64]{3,1,2,0:T(8,128)(2,1)S(1)}, bf16[4,32,2,64]{3,1,2,0:T(8,128)(2,1)}, u32[]{:S(2)}) copy-start(bf16[4,32,2,64]{3,1,2,0:T(8,128)(2,1)} %copy-done.11) | copy-start | bytes 98308
  77.2 5.3 %copy-start.3 = (f32[32,32,2,8]{0,1,3,2:T(8,128)S(1)}, f32[32,32,2,8]{0,1,3,2:T(8,128)}, u32[]{:S(2)}) copy-start(f32[32,32,2,8]{0,1,3,2:T(8,128)} %copy.224) | copy-start | bytes 196612
  83.2 1.9 copy-start.13
  84.2 49.3 %copy-start.15 = (f32[1,1024]{1,0:T(1,128)S(1)}, f32[1,1024]{1,0:T(1,128)}, u32[]{:S(2)}) copy-start(f32[1,1024]{1,0:T(1,128)} %get-tuple-element.32) | copy-start | bytes 12292
  85.1 92.1 %reduce-scatter.12.cloned.1.call-start = ((), (), s32[]{:S(2)}) async-start(), calls=%async_computation.5 | async-start | bytes 294912
  88.7 45.0 %copy-start.7 = (bf16[1,16,64,128]{3,2,0,1:T(8,128)(2,1)S(1)}, bf16[1,16,64,128]{3,2,0,1:T(8,128)(2,1)}, u32[]{:S(2)}) copy-start(bf16[1,16,64,128]{3,2,0,1:T(8,128)(2,1)} %get-tuple-element.16) | copy-start | bytes 786436
  89.5 45.2 %copy-start.8 = (bf16[1,16,64,128]{3,2,0,1:T(8,128)(2,1)S(1)}, bf16[1,16,64,128]{3,2,0,1:T(8,128)(2,1)}, u32[]{:S(2)}) copy-start(bf16[1,16,64,128]{3,2,0,1:T(8,128)(2,1)} %get-tuple-element.19) | copy-start | bytes 786436
  126.3 13.5 %copy-start.9 = (bf16[1,16,64,128]{3,2,0,1:T(8,128)(2,1)S(1)}, bf16[1,16,64,128]{3,2,0,1:T(8,128)(2,1)}, u32[]{:S(2)}) copy-start(bf16[1,16,64,128]{3,2,0,1:T(8,128)(2,1)} %get-tuple-element.13) | copy-start | bytes 786436
  135.2 5.5 %collective-permute-start.4 = (bf16[4,32,2,128]{3,1,2,0:T(8,128)(2,1)S(1)}, bf16[4,32,2,128]{3,1,2,0:T(8,128)(2,1)S(1)}, u32[]{:S(2)}, u32[]{:S(2)}) collective-permute-start(bf16[4,32,2,128]{3,1,2,0:T(8,128)(2,1)S(1)} %pad_maximum_fusion.5), channel_id=1, source_target_pairs={{0,8},{8,16},{16,24},{24,32},{32,40},{40,48},{48,56},{56,64},{64,7... | collective-permute-start | bytes 196616 | tf_op jit(solution)/shard_map/ppermute | solution.py:25
  138.3 5.0 %collective-permute-start.5 = (bf16[4,32,2,128]{3,1,2,0:T(8,128)(2,1)S(1)}, bf16[4,32,2,128]{3,1,2,0:T(8,128)(2,1)S(1)}, u32[]{:S(2)}, u32[]{:S(2)}) collective-permute-start(bf16[4,32,2,128]{3,1,2,0:T(8,128)(2,1)S(1)} %pad_maximum_fusion.5), channel_id=1, source_target_pairs={{8,0},{16,8},{24,16},{32,24},{40,32},{48,40},{56,48},{64,56},{72,6... | collective-permute-start | bytes 196616 | tf_op jit(solution)/shard_map/ppermute | solution.py:26
  146.2 92.6 %reduce-scatter.14.cloned.1.call-start = ((), (), s32[]{:S(2)}) async-start(), calls=%async_computation.6 | async-start | bytes 294912
  149.9 45.7 %copy-start.4 = (bf16[1,16,64,128]{3,2,0,1:T(8,128)(2,1)S(1)}, bf16[1,16,64,128]{3,2,0,1:T(8,128)(2,1)}, u32[]{:S(2)}) copy-start(bf16[1,16,64,128]{3,2,0,1:T(8,128)(2,1)} %get-tuple-element.15) | copy-start | bytes 786436
  150.6 45.8 %copy-start.5 = (bf16[1,16,64,128]{3,2,0,1:T(8,128)(2,1)S(1)}, bf16[1,16,64,128]{3,2,0,1:T(8,128)(2,1)}, u32[]{:S(2)}) copy-start(bf16[1,16,64,128]{3,2,0,1:T(8,128)(2,1)} %get-tuple-element.18) | copy-start | bytes 786436
  188.0 13.3 %copy-start.6 = (bf16[1,16,64,128]{3,2,0,1:T(8,128)(2,1)S(1)}, bf16[1,16,64,128]{3,2,0,1:T(8,128)(2,1)}, u32[]{:S(2)}) copy-start(bf16[1,16,64,128]{3,2,0,1:T(8,128)(2,1)} %get-tuple-element.12) | copy-start | bytes 786436
  196.9 5.3 %collective-permute-start.6 = (bf16[4,32,2,128]{3,1,2,0:T(8,128)(2,1)S(1)}, bf16[4,32,2,128]{3,1,2,0:T(8,128)(2,1)S(1)}, u32[]{:S(2)}, u32[]{:S(2)}) collective-permute-start(bf16[4,32,2,128]{3,1,2,0:T(8,128)(2,1)S(1)} %pad_maximum_fusion.6), channel_id=1, source_target_pairs={{0,8},{8,16},{16,24},{24,32},{32,40},{40,48},{48,56},{56,64},{64,7... | collective-permute-start | bytes 196616 | tf_op jit(solution)/shard_map/ppermute | solution.py:25
  200.0 5.0 %collective-permute-start.7 = (bf16[4,32,2,128]{3,1,2,0:T(8,128)(2,1)S(1)}, bf16[4,32,2,128]{3,1,2,0:T(8,128)(2,1)S(1)}, u32[]{:S(2)}, u32[]{:S(2)}) collective-permute-start(bf16[4,32,2,128]{3,1,2,0:T(8,128)(2,1)S(1)} %pad_maximum_fusion.6), channel_id=1, source_target_pairs={{8,0},{16,8},{24,16},{32,24},{40,32},{48,40},{56,48},{64,56},{72,6... | collective-permute-start | bytes 196616 | tf_op jit(solution)/shard_map/ppermute | solution.py:26
Sparse Core Ops, SparseCore 0:
  9.5 49.5 all-gather.5
  85.2 30.1 reduce-scatter.9
  146.3 30.7 reduce-scatter.11
  207.9 30.7 reduce-scatter.13
where the time goes:
time: 250 us; the launch traced here: 247 us
  waiting for transfers between devices  110 us (44%)
  blocking collectives  49.2 us (20%)
  local copies, waits for them, and re-layouts  38.1 us (15%)
  starting transfers between devices  19.3 us (8%)
  between operations  14.2 us (6%)
  other arithmetic  10.2 us (4%)
  matrix products  6.03 us (2%)
    unnamed x7, waiting for transfers between devices  83.1 us
    all_gather x6, blocking collectives, stacked_from(): blocks = lax.all_gather(blocks, axes[k], axis=0, tiled=True)  49.2 us
    all_gather x1, waiting for transfers between devices, gather_together(): lines, at, done = (lax.all_gather(ravelled, axis), 0, [])  21.3 us
    ppermute x4, starting transfers between devices, with_halo(): before = lax.ppermute(last, axis, up)  13.8 us
    gather x6, local copies, waits for them, and re-layouts, attend(): bias_table = bias_layer[:, :, jnp.clip(col_offset, 0, WIN_COLS - 1)]  13.4 us
    unnamed x75, local copies, waits for them, and re-layouts  9.4 us
    ppermute x4, waiting for transfers between devices, with_halo(): after = lax.ppermute(leading, axis, down)  5.46 us
    ppermute x4, starting transfers between devices, with_halo(): after = lax.ppermute(leading, axis, down)  5.34 us
  transfers between devices with their start and end apart: 12, of which 6 were waited for; matrix products, arithmetic and copies ran while one was open for 10% of the time, Pallas kernels for 0%

commit v1 on v0

v1 whole, which is shorter than its diff:
```python
import jax
import jax.numpy as jnp
from jax import lax
from jax.experimental import pallas as pl
from jax.experimental.pallas import tpu as pltpu
from jax.sharding import PartitionSpec as P

MESH = pl.DeviceIdType.MESH
LAYERS = 3
EPS = 1e-06
NEG = -1e30
BF = jnp.bfloat16
F32 = jnp.float32

RING = (2, 1, 3)
TP_PEERS = ((2, 0), (2, 1), (1, 0), (3, 0), (1, 1), (3, 1), (0, 1))

N_AG = 7
N_W = 12
N_HALO = 2
N_RS = 7
AG0 = 0
W0 = AG0 + LAYERS * N_AG
HALO0 = W0 + LAYERS * N_W
RS0 = HALO0 + LAYERS * N_HALO
DOC0 = RS0 + LAYERS * N_RS
N_COPIES = DOC0 + 2


def kernel(
    tok_ref, gain_ref, wq_ref, wk_ref, wv_ref, wo_ref, bias_ref, docs_ref, out_ref,
    W, G, KV, DOC, R, S, BM, PB, ssem, rsem, lsem,
):
    s = lax.axis_index("sp")
    t = lax.axis_index("tp")
    z, x = s // 4, s % 4
    y, c = t // 2, t % 2
    sends = []

    def rdma(src, dst, sem, device):
        copy = pltpu.make_async_remote_copy(
            src_ref=src,
            dst_ref=dst,
            send_sem=ssem.at[sem],
            recv_sem=rsem.at[sem],
            device_id=device,
            device_id_type=MESH,
        )
        copy.start()
        sends.append(copy)
        return copy

    def tp_peer(dy, dc):
        return ((y + dy) % 4) * 2 + (c + dc) % 2

    local = [
        pltpu.make_async_copy(tok_ref, G.at[0, t], lsem.at[0]),
        pltpu.make_async_copy(docs_ref, DOC.at[1], lsem.at[1]),
        pltpu.make_async_copy(wq_ref, W.at[:, 0, z, x], lsem.at[2]),
        pltpu.make_async_copy(wk_ref, W.at[:, 1, z, x], lsem.at[3]),
        pltpu.make_async_copy(wv_ref, W.at[:, 2, z, x], lsem.at[4]),
    ]
    for copy in local:
        copy.start()

    barrier = pltpu.get_barrier_semaphore()
    for k in range(1, 16):
        pl.semaphore_signal(barrier, inc=1, device_id={"sp": (s + k) % 16}, device_id_type=MESH)
    for k in range(1, 8):
        pl.semaphore_signal(barrier, inc=1, device_id={"tp": (t + k) % 8}, device_id_type=MESH)

    for l in range(LAYERS):
        W[l, 3, z, x] = wo_ref[l].astype(F32).T.astype(BF)
    PB[...] = jnp.zeros_like(PB)

    for copy in local:
        copy.wait()
    pl.semaphore_wait(barrier, 22)

    def gather_tp(l):
        return [
            rdma(G.at[l, t], G.at[l, t], AG0 + l * N_AG + i, {"tp": tp_peer(dy, dc)})
            for i, (dy, dc) in enumerate(TP_PEERS)
        ]

    nxt, prv = (s + 1) % 16, (s + 15) % 16
    gathers = gather_tp(0)
    doc_copies = [
        rdma(DOC.at[1], DOC.at[0], DOC0, {"sp": nxt}),
        rdma(DOC.at[1], DOC.at[2], DOC0 + 1, {"sp": prv}),
    ]

    def phase_one(l):
        base = W0 + l * N_W
        along_x = [
            rdma(W.at[l, 0:2, z, x], W.at[l, 0:2, z, x], base + i, {"sp": z * 4 + (x + d) % 4})
            for i, d in enumerate(RING)
        ]
        along_z = [
            rdma(W.at[l, 2:4, z, x], W.at[l, 2:4, z, x], base + 3 + i, {"sp": ((z + d) % 4) * 4 + x})
            for i, d in enumerate(RING)
        ]
        return along_x, along_z

    def phase_two(l, first):
        base = W0 + l * N_W + 6
        along_x, along_z = first
        for copy in along_x:
            copy.wait_recv()
        then_z = [
            rdma(W.at[l, 0:2, z], W.at[l, 0:2, z], base + i, {"sp": ((z + d) % 4) * 4 + x})
            for i, d in enumerate(RING)
        ]
        for copy in along_z:
            copy.wait_recv()
        then_x = [
            rdma(W.at[l, 2:4, :, x], W.at[l, 2:4, :, x], base + 3 + i, {"sp": z * 4 + (x + d) % 4})
            for i, d in enumerate(RING)
        ]
        return then_z + then_x

    firsts = [phase_one(l) for l in range(LAYERS)]
    weights = [phase_two(l, firsts[l]) for l in range(LAYERS)]

    for copy in doc_copies:
        copy.wait_recv()
    qi = lax.broadcasted_iota(jnp.int32, (128, 384), 0)
    kj = lax.broadcasted_iota(jnp.int32, (128, 384), 1)
    row_off = (kj >> 5) - (qi >> 5)
    col_off = (kj & 31) - (qi & 31) + 8
    key_docs = jnp.concatenate([DOC[0], DOC[1], DOC[2]], axis=1)
    eye = lax.broadcasted_iota(jnp.int32, (128, 128), 0) == lax.broadcasted_iota(jnp.int32, (128, 128), 1)
    own_docs = jnp.sum(
        jnp.where(eye, jnp.broadcast_to(DOC[1], (128, 128)).astype(F32), 0.0), axis=1, keepdims=True
    )
    lowest = jnp.where(s > 0, 0, 128)
    highest = jnp.where(s < 15, 384, 256)
    allowed = (
        (row_off >= 0) & (row_off < 8) & (col_off >= 0) & (col_off < 16)
        & (key_docs.astype(F32) == own_docs) & (kj >= lowest) & (kj < highest)
    )
    lines = jnp.zeros((6, 512), F32)
    for a in range(8):
        PB[:, 0:16] = bias_ref[:, a, :]
        lines += pltpu.roll(PB[...], 119 + 32 * a, 1)
    for l in range(LAYERS):
        for h in range(2):
            line = jnp.broadcast_to(lines[l * 2 + h : l * 2 + h + 1], (128, 512))
            table = pltpu.roll(line, 385, 1, stride=1, stride_axis=0)
            BM[l, pl.ds(h * 128, 128), :] = jnp.where(allowed, table[:, :384], NEG)

    lane = lax.broadcasted_iota(jnp.int32, (128, 128), 1)
    left = lane < 64

    def head_norm(raw):
        values = raw.astype(BF).astype(F32)
        squares = values * values
        total0 = jnp.sum(jnp.where(left, squares, 0.0), axis=1, keepdims=True)
        total1 = jnp.sum(jnp.where(left, 0.0, squares), axis=1, keepdims=True)
        mean = jnp.where(left, total0, total1) * (1.0 / 64)
        return values * lax.rsqrt(mean + EPS)

    for l in range(LAYERS):
        for copy in gathers:
            copy.wait_recv()
        total = jnp.zeros((128, 1), F32)
        for i in range(8):
            part = G[l, i].astype(F32)
            total += jnp.sum(part * part, axis=1, keepdims=True)
        scale = lax.rsqrt(total * (1.0 / 1024) + EPS)
        normed = jnp.concatenate(
            [
                (G[l, i].astype(F32) * scale * gain_ref[l : l + 1, i * 128 : (i + 1) * 128]).astype(BF)
                for i in range(8)
            ],
            axis=1,
        )
        for copy in weights[l]:
            copy.wait_recv()
        wk = W[l, 1].reshape(1024, 128)
        wv = W[l, 2].reshape(1024, 128)
        key_raw = jnp.dot(normed, wk, preferred_element_type=F32)
        value_raw = jnp.dot(normed, wv, preferred_element_type=F32)
        KV[l, 1, 0] = head_norm(key_raw).astype(BF)
        KV[l, 1, 1] = value_raw.astype(BF)
        halos = [
            rdma(KV.at[l, 1], KV.at[l, 0], HALO0 + l * N_HALO, {"sp": nxt}),
            rdma(KV.at[l, 1], KV.at[l, 2], HALO0 + l * N_HALO + 1, {"sp": prv}),
        ]
        wq = W[l, 0].reshape(1024, 128)
        query = head_norm(jnp.dot(normed, wq, preferred_element_type=F32)).astype(BF)
        query = query * jnp.asarray(0.125, BF)
        zero = jnp.zeros_like(query)
        query = jnp.concatenate([jnp.where(left, query, zero), jnp.where(left, zero, query)], axis=0)
        for copy in halos:
            copy.wait_recv()
        keys = KV[l, :, 0].reshape(384, 128)
        values = KV[l, :, 1].reshape(384, 128)
        scores = lax.dot_general(
            query, keys, (((1,), (1,)), ((), ())), preferred_element_type=F32
        ) + BM[l]
        probs = jnp.exp(scores - jnp.max(scores, axis=1, keepdims=True))
        norm = jnp.sum(probs, axis=1, keepdims=True)
        mixed = jnp.dot(probs.astype(BF), values, preferred_element_type=F32) / norm
        attended = jnp.where(left, mixed[:128], mixed[128:]).astype(BF)
        partial = lax.dot_general(
            attended, W[l, 3].reshape(1024, 128), (((1,), (1,)), ((), ())), preferred_element_type=F32
        ).astype(BF)
        for i in range(8):
            S[l, i] = partial[:, i * 128 : (i + 1) * 128]
        reduces = []
        for i, (dy, dc) in enumerate(TP_PEERS):
            peer = tp_peer(dy, dc)
            reduces.append(rdma(S.at[l, peer], R.at[l, i], RS0 + l * N_RS + i, {"tp": peer}))
        result = S[l, t].astype(F32)
        for i, copy in enumerate(reduces):
            copy.wait_recv()
            result += R[l, i].astype(F32)
        if l < LAYERS - 1:
            G[l + 1, t] = result.astype(BF)
            gathers = gather_tp(l + 1)
        else:
            out_ref[...] = result.astype(BF)

    for copy in sends:
        copy.wait_send()


def local(tokens, norm_gain, w_query, w_key, w_value, w_out, offset_bias, documents):
    vmem = pl.BlockSpec(memory_space=pltpu.VMEM)
    hbm = pl.BlockSpec(memory_space=pl.ANY)
    return pl.pallas_call(
        kernel,
        out_shape=jax.ShapeDtypeStruct((128, 128), BF),
        in_specs=[hbm, vmem, hbm, hbm, hbm, vmem, vmem, hbm],
        out_specs=vmem,
        scratch_shapes=[
            pltpu.VMEM((LAYERS, 4, 4, 4, 64, 128), BF),
            pltpu.VMEM((LAYERS, 8, 128, 128), BF),
            pltpu.VMEM((LAYERS, 3, 2, 128, 128), BF),
            pltpu.VMEM((3, 1, 128), jnp.int32),
            pltpu.VMEM((LAYERS, 7, 128, 128), BF),
            pltpu.VMEM((LAYERS, 8, 128, 128), BF),
            pltpu.VMEM((LAYERS, 256, 384), F32),
            pltpu.VMEM((6, 512), F32),
            pltpu.SemaphoreType.DMA((N_COPIES,)),
            pltpu.SemaphoreType.DMA((N_COPIES,)),
            pltpu.SemaphoreType.DMA((5,)),
        ],
        compiler_params=pltpu.CompilerParams(collective_id=0, has_side_effects=True),
    )(
        tokens, norm_gain, w_query, w_key, w_value, w_out,
        offset_bias.reshape(2 * LAYERS, 8, 16), documents.reshape(1, 128),
    )


def solution(mesh):
    return jax.shard_map(
        local,
        mesh=mesh,
        in_specs=(
            P("sp", "tp"),
            P(),
            P(None, "sp", "tp"),
            P(None, "sp", "tp"),
            P(None, "sp", "tp"),
            P(None, "tp", "sp"),
            P(None, "tp", None, None),
            P("sp"),
        ),
        out_specs=P("sp", "tp"),
        check_vma=False,
    )
```

time: 250 us -> 77.4 us (0.31); the launches traced: 247 us -> 77 us
  waiting for transfers between devices: 110 us -> 0 us
  Pallas kernels: 0 us -> 74.1 us
  blocking collectives: 49.2 us -> 0 us
  local copies, waits for them, and re-layouts: 38.1 us -> 2.9 us
  starting transfers between devices: 19.3 us -> 0 us
  between operations: 14.2 us -> 0.01 us
  other arithmetic: 10.2 us -> 0 us
  matrix products: 6.03 us -> 0 us
    unnamed x7 -> x0, waiting for transfers between devices: 83.1 us -> none
    pallas_call x0 -> x1, Pallas kernels: none -> 74.1 us  [local(): pl.pallas_call(kernel, out_shape=jax.ShapeDtypeStruct((128, 128), BF), in...]
    all_gather x6 -> x0, blocking collectives: 49.2 us -> none  [stacked_from(): blocks = lax.all_gather(blocks, axes[k], axis=0, tiled=True)]
    all_gather x1 -> x0, waiting for transfers between devices: 21.3 us -> none  [gather_together(): lines, at, done = (lax.all_gather(ravelled, axis), 0, [])]
    ppermute x8 -> x0, starting transfers between devices: 19.2 us -> none  [the longest x4 13.8 us: with_halo(): before = lax.ppermute(last, axis, up)]
    gather x6 -> x0, local copies, waits for them, and re-layouts: 13.4 us -> none  [attend(): bias_table = bias_layer[:, :, jnp.clip(col_offset, 0, WIN_COLS - 1)]]
    slice x10 -> x0, local copies, waits for them, and re-layouts: 7.95 us -> none  [the longest x4 2.63 us: local(): collected[3][layer_index]]
    unnamed x75 -> x2, local copies, waits for them, and re-layouts: 9.4 us -> 2.9 us
  transfers between devices with their start and end apart: 12 -> 0, of which waited for: 6 -> 0; matrix products, arithmetic and copies ran while one was open for 10% -> 0% of each run, Pallas kernels for 0% -> 0%
where the time goes in v1:
time: 77.4 us; the launch traced here: 77 us
  Pallas kernels  74.1 us (96%)
  local copies, waits for them, and re-layouts  2.9 us (4%)
    pallas_call x1, Pallas kernels, local(): pl.pallas_call(kernel, out_shape=jax.ShapeDtypeStruct((128, 128), BF), in...  74.1 us
    unnamed x2, local copies, waits for them, and re-layouts  2.9 us

profile of v1, /device:TPU:1, one launch (start us, length us, event | category | flops | bytes accessed | tf_op | source)
XLA Modules:
  0.0 77.0 jit_solution(8402029010125024955)
XLA Ops:
  0.0 1.5 %copy.9.wo_ref = bf16[3,128,64]{2,1,0:T(8,128)(2,1)} copy(bf16[3,128,64]{1,2,0:T(8,128)(2,1)} %param.13) | data formatting | bytes 98304 | tf_op args[5]
  1.5 74.1 %shard_map.82 = bf16[128,128]{1,0:T(8,128)(2,1)} custom-call(bf16[128,128]{1,0:T(8,128)(2,1)} %tok_ref.1, f32[3,1024]{1,0:T(4,128)} %gain_ref.1, bf16[3,64,128]{2,1,0:T(8,128)(2,1)} %wq_ref.1, bf16[3,64,128]{2,1,0:T(8,128)(2,1)} %wk_ref.1, bf16[3,64,128]{2,1,0:T(8,128)(2,1)} %wv_ref.1, bf16[3,128,64]{2,1,0:T(8,128)(2,1)} %copy.9.wo_ref, ...), custom_call_target="tpu_custom_call" | custom-call | tf_op jit(solution)/shard_map/pallas_call | solution.py:232
  75.7 1.4 %copy.11 = bf16[128,128]{1,0:T(8,128)(2,1)} copy(bf16[128,128]{1,0:T(8,128)(2,1)} %shard_map.82) | data formatting | bytes 65536

commit v2 on v1

v2 whole, which is shorter than its diff:
```python
import jax
import jax.numpy as jnp
from jax import lax
from jax.experimental import pallas as pl
from jax.experimental.pallas import tpu as pltpu
from jax.sharding import PartitionSpec as P

MESH = pl.DeviceIdType.MESH
LAYERS = 3
EPS = 1e-06
NEG = -1e30
BF = jnp.bfloat16
F32 = jnp.float32

RING = (2, 1, 3)
TP_PEERS = ((2, 0), (2, 1), (1, 0), (3, 0), (1, 1), (3, 1), (0, 1))
Y_FIRST = 32
N_COPIES = 160


def kernel(
    tok_ref, gain_ref, wq_ref, wk_ref, wv_ref, wo_ref, bias_ref, docs_ref, out_ref,
    W, WO, WL, G, A, KV, DOC, R, S, RX, SX, BM, PB, ssem, rsem, lsem,
):
    s = lax.axis_index("sp")
    t = lax.axis_index("tp")
    z, x = s // 4, s % 4
    y, c = t // 2, t % 2
    sends = []

    def rdma(src, dst, device):
        sem = len(sends)
        copy = pltpu.make_async_remote_copy(
            src_ref=src,
            dst_ref=dst,
            send_sem=ssem.at[sem],
            recv_sem=rsem.at[sem],
            device_id=device,
            device_id_type=MESH,
        )
        copy.start()
        sends.append(copy)
        return copy

    def arrive(name, copies):
        with jax.named_scope(name):
            for copy in copies:
                copy.wait_recv()

    def x_peer(d):
        return {"sp": z * 4 + (x + d) % 4}

    def z_peer(d):
        return {"sp": ((z + d) % 4) * 4 + x}

    def y_peer(d):
        return {"tp": ((y + d) % 4) * 2 + c}

    def tp_peer(dy, dc):
        return ((y + dy) % 4) * 2 + (c + dc) % 2

    nxt, prv = {"sp": (s + 1) % 16}, {"sp": (s + 15) % 16}
    partner = {"tp": y * 2 + 1 - c}

    local = [
        pltpu.make_async_copy(tok_ref, G.at[t], lsem.at[0]),
        pltpu.make_async_copy(docs_ref, DOC.at[1], lsem.at[1]),
        pltpu.make_async_copy(wq_ref, W.at[:, 0, z, x], lsem.at[2]),
        pltpu.make_async_copy(wk_ref, W.at[:, 1, z, x], lsem.at[3]),
        pltpu.make_async_copy(wv_ref, W.at[:, 2, z, x], lsem.at[4]),
        pltpu.make_async_copy(wo_ref.at[0:2], WO.at[:, y, z, x], lsem.at[5]),
        pltpu.make_async_copy(wo_ref.at[2], WL.at[z, x], lsem.at[6]),
    ]
    with jax.named_scope("init"):
        for copy in local:
            copy.start()

    barrier = pltpu.get_barrier_semaphore()
    greeted = [x_peer(d) for d in RING] + [z_peer(d) for d in RING] + [nxt, prv]
    greeted += [{"tp": tp_peer(dy, dc)} for dy, dc in TP_PEERS]
    for device in greeted:
        pl.semaphore_signal(barrier, inc=1, device_id=device, device_id_type=MESH)

    PB[...] = jnp.zeros_like(PB)
    for l in range(LAYERS):
        KV[l, :, 352:384, :] = jnp.zeros((2, 32, 128), BF)

    with jax.named_scope("wait_local"):
        for copy in local:
            copy.wait()
    with jax.named_scope("wait_barrier"):
        pl.semaphore_wait(barrier, len(greeted))

    def block_one(ref, rows_a, rows_b):
        along_x = [rdma(ref(z, x, rows_a), ref(z, x, rows_a), x_peer(d)) for d in RING]
        along_z = [rdma(ref(z, x, rows_b), ref(z, x, rows_b), z_peer(d)) for d in RING]
        return along_x + along_z

    def block_two(ref, rows_a, rows_b):
        every = slice(None)
        then_z = [rdma(ref(z, every, rows_a), ref(z, every, rows_a), z_peer(d)) for d in RING]
        then_x = [rdma(ref(every, x, rows_b), ref(every, x, rows_b), x_peer(d)) for d in RING]
        return then_z + then_x

    def halves(low, high):
        mid = (low + high) // 2
        return slice(low, mid), slice(mid, high)

    class Gather:
        def __init__(self, name, ref, low, high):
            self.name, self.ref, self.rows = name, ref, halves(low, high)

        def one(self):
            self.first = block_one(self.ref, *self.rows)

        def two(self):
            arrive("p1_" + self.name, self.first)
            self.second = block_two(self.ref, *self.rows)

        def done(self):
            arrive("p2_" + self.name, self.second)

    qkv = [
        Gather(f"qkv{l}", lambda i, j, rows, l=l: W.at[l, :, i, j, rows], 0, 64)
        for l in range(LAYERS)
    ]
    out_y = [
        Gather(f"oy{l}", lambda i, j, rows, l=l: WO.at[l, :, i, j, rows], 0, Y_FIRST)
        for l in range(LAYERS - 1)
    ]
    out_p = [
        Gather(f"op{l}", lambda i, j, rows, l=l: WO.at[l, y, i, j, rows], Y_FIRST, 64)
        for l in range(LAYERS - 1)
    ]
    out_last = Gather("ol", lambda i, j, rows: WL.at[i, j, rows], 0, 64)

    def cross_y_first(l):
        ref = WO.at[l, y, z, x, 0:Y_FIRST]
        return [rdma(ref, ref, y_peer(d)) for d in RING]

    def cross_y_last(l):
        ref = WO.at[l, y, :, :, Y_FIRST:64]
        return [rdma(ref, ref, y_peer(d)) for d in RING]

    gathers = [rdma(G.at[t], G.at[t], {"tp": tp_peer(dy, dc)}) for dy, dc in TP_PEERS]
    doc_copies = [rdma(DOC.at[1], DOC.at[0], nxt), rdma(DOC.at[1], DOC.at[2], prv)]
    qkv[0].one()
    crossed = [cross_y_first(l) for l in range(LAYERS - 1)]
    crossed_last = [None, None]
    out_p[0].one()

    arrive("docs", doc_copies)
    qi = lax.broadcasted_iota(jnp.int32, (128, 384), 0)
    kj = lax.broadcasted_iota(jnp.int32, (128, 384), 1)
    row_off = (kj >> 5) - (qi >> 5)
    col_off = (kj & 31) - (qi & 31) + 8
    key_docs = jnp.concatenate([DOC[0], DOC[1], DOC[2]], axis=1)
    eye = lax.broadcasted_iota(jnp.int32, (128, 128), 0) == lax.broadcasted_iota(jnp.int32, (128, 128), 1)
    own_docs = jnp.sum(
        jnp.where(eye, jnp.broadcast_to(DOC[1], (128, 128)).astype(F32), 0.0), axis=1, keepdims=True
    )
    lowest = jnp.where(s > 0, 0, 128)
    highest = jnp.where(s < 15, 384, 256)
    allowed = (
        (row_off >= 0) & (row_off < 8) & (col_off >= 0) & (col_off < 16)
        & (key_docs.astype(F32) == own_docs) & (kj >= lowest) & (kj < highest)
    )
    lines = jnp.zeros((6, 512), F32)
    for a in range(8):
        PB[:, 0:16] = bias_ref[:, a, :]
        lines += pltpu.roll(PB[...], 119 + 32 * a, 1)
    for l in range(LAYERS):
        for h in range(2):
            line = jnp.broadcast_to(lines[l * 2 + h : l * 2 + h + 1], (128, 512))
            table = pltpu.roll(line, 385, 1, stride=1, stride_axis=0)
            BM[l, pl.ds(h * 128, 128), :] = jnp.where(allowed, table[:, :384], NEG)

    lane = lax.broadcasted_iota(jnp.int32, (128, 128), 1)
    left = lane < 64

    def head_norm(raw):
        values = raw.astype(BF).astype(F32)
        squares = values * values
        total0 = jnp.sum(jnp.where(left, squares, 0.0), axis=1, keepdims=True)
        total1 = jnp.sum(jnp.where(left, 0.0, squares), axis=1, keepdims=True)
        mean = jnp.where(left, total0, total1) * (1.0 / 64)
        return values * lax.rsqrt(mean + EPS)

    qkv[0].two()
    arrive("cross0", crossed[0])
    out_y[0].one()

    for l in range(LAYERS):
        if l == 0:
            arrive("gather0", gathers)
            stream = [G[i].astype(F32) for i in range(8)]
        else:
            arrive(f"gather{l}", gathers)
            attended = jnp.concatenate([A[l - 1, i] for i in range(4)], axis=1)
            out_y[l - 1].done()
            arrive(f"cross_last{l}", crossed_last[l - 1])
            exchanges, parts = [], []
            for half in range(2):
                weight = jnp.concatenate(
                    [WO[l - 1, i, 2 * half : 2 * half + 2].reshape(512, 128) for i in range(4)], axis=1
                )
                part = lax.dot_general(
                    attended, weight, (((1,), (1,)), ((), ())), preferred_element_type=F32
                )
                SX[l - 1, half] = part.astype(BF)
                exchanges.append(rdma(SX.at[l - 1, half], RX.at[l - 1, half], partner))
                parts.append(part)
            stream = []
            for half in range(2):
                arrive(f"exchange{l}_{half}", exchanges[half : half + 1])
                whole = (parts[half] + RX[l - 1, half].astype(F32)).astype(BF).astype(F32)
                stream += [whole[:, i * 128 : (i + 1) * 128] for i in range(4)]
        total = jnp.zeros((128, 1), F32)
        for part in stream:
            total += jnp.sum(part * part, axis=1, keepdims=True)
        scale = lax.rsqrt(total * (1.0 / 1024) + EPS)
        normed = jnp.concatenate(
            [
                (part * scale * gain_ref[l : l + 1, i * 128 : (i + 1) * 128]).astype(BF)
                for i, part in enumerate(stream)
            ],
            axis=1,
        )
        qkv[l].done()
        key_raw = jnp.dot(normed, W[l, 1].reshape(1024, 128), preferred_element_type=F32)
        value_raw = jnp.dot(normed, W[l, 2].reshape(1024, 128), preferred_element_type=F32)
        KV[l, 0, 128:256] = head_norm(key_raw).astype(BF)
        KV[l, 1, 128:256] = value_raw.astype(BF)
        halos = [
            rdma(KV.at[l, :, 128:256], KV.at[l, :, 0:128], nxt),
            rdma(KV.at[l, :, 128:224], KV.at[l, :, 256:352], prv),
        ]
        if l == 0:
            qkv[1].one()
            out_p[0].two()
            out_y[0].two()
        elif l == 1:
            qkv[2].one()
            out_p[1].two()
            out_y[1].two()
        query = head_norm(
            jnp.dot(normed, W[l, 0].reshape(1024, 128), preferred_element_type=F32)
        ).astype(BF)
        query = query * jnp.asarray(0.125, BF)
        zero = jnp.zeros_like(query)
        query = jnp.concatenate([jnp.where(left, query, zero), jnp.where(left, zero, query)], axis=0)
        arrive(f"halo{l}", halos)
        scores = lax.dot_general(
            query, KV[l, 0], (((1,), (1,)), ((), ())), preferred_element_type=F32
        ) + BM[l]
        probs = jnp.exp(scores - jnp.max(scores, axis=1, keepdims=True))
        norm = jnp.sum(probs, axis=1, keepdims=True)
        mixed = jnp.dot(probs.astype(BF), KV[l, 1], preferred_element_type=F32) / norm
        heads = jnp.where(left, mixed[:128], mixed[128:]).astype(BF)
        if l < LAYERS - 1:
            A[l, y] = heads
            gathers = [rdma(A.at[l, y], A.at[l, y], y_peer(d)) for d in RING]
            qkv[l + 1].two()
            out_p[l].done()
            crossed_last[l] = cross_y_last(l)
            if l == 0:
                out_p[1].one()
                arrive("cross1", crossed[1])
                out_y[1].one()
                out_last.one()
            else:
                out_last.two()
            continue
        out_last.done()
        partial = lax.dot_general(
            heads, WL[...].reshape(1024, 128), (((1,), (1,)), ((), ())), preferred_element_type=F32
        ).astype(BF)
        for i in range(8):
            S[i] = partial[:, i * 128 : (i + 1) * 128]
        reduces = []
        for i, (dy, dc) in enumerate(TP_PEERS):
            peer = tp_peer(dy, dc)
            reduces.append(rdma(S.at[peer], R.at[i], {"tp": peer}))
        result = S[t].astype(F32)
        arrive("reduce", reduces)
        for i in range(7):
            result += R[i].astype(F32)
        out_ref[...] = result.astype(BF)

    with jax.named_scope("wait_sends"):
        for copy in sends:
            copy.wait_send()


def local(tokens, norm_gain, w_query, w_key, w_value, w_out, offset_bias, documents):
    vmem = pl.BlockSpec(memory_space=pltpu.VMEM)
    hbm = pl.BlockSpec(memory_space=pl.ANY)
    return pl.pallas_call(
        kernel,
        out_shape=jax.ShapeDtypeStruct((128, 128), BF),
        in_specs=[hbm, vmem, hbm, hbm, hbm, hbm, vmem, hbm],
        out_specs=vmem,
        scratch_shapes=[
            pltpu.VMEM((LAYERS, 3, 4, 4, 64, 128), BF),
            pltpu.VMEM((LAYERS - 1, 4, 4, 4, 64, 128), BF),
            pltpu.VMEM((4, 4, 64, 128), BF),
            pltpu.VMEM((8, 128, 128), BF),
            pltpu.VMEM((LAYERS - 1, 4, 128, 128), BF),
            pltpu.VMEM((LAYERS, 2, 384, 128), BF),
            pltpu.VMEM((3, 1, 128), jnp.int32),
            pltpu.VMEM((7, 128, 128), BF),
            pltpu.VMEM((8, 128, 128), BF),
            pltpu.VMEM((LAYERS - 1, 2, 128, 512), BF),
            pltpu.VMEM((LAYERS - 1, 2, 128, 512), BF),
            pltpu.VMEM((LAYERS, 256, 384), F32),
            pltpu.VMEM((6, 512), F32),
            pltpu.SemaphoreType.DMA((N_COPIES,)),
            pltpu.SemaphoreType.DMA((N_COPIES,)),
            pltpu.SemaphoreType.DMA((7,)),
        ],
        compiler_params=pltpu.CompilerParams(collective_id=0, has_side_effects=True),
    )(
        tokens, norm_gain, w_query, w_key, w_value, jnp.swapaxes(w_out, 1, 2),
        offset_bias.reshape(2 * LAYERS, 8, 16), documents.reshape(1, 128),
    )


def solution(mesh):
    return jax.shard_map(
        local,
        mesh=mesh,
        in_specs=(
            P("sp", "tp"),
            P(),
            P(None, "sp", "tp"),
            P(None, "sp", "tp"),
            P(None, "sp", "tp"),
            P(None, "tp", "sp"),
            P(None, "tp", None, None),
            P("sp"),
        ),
        out_specs=P("sp", "tp"),
        check_vma=False,
    )
```

time: 77.4 us -> 67.8 us (0.88)
  Pallas kernels: 74.1 us -> 66.2 us
  local copies, waits for them, and re-layouts: 2.9 us -> 1.38 us
    pallas_call x1, Pallas kernels: 74.1 us -> 66.2 us  [local(): pl.pallas_call(kernel, out_shape=jax.ShapeDtypeStruct((128, 128), BF), in...]
    unnamed x2 -> x1, local copies, waits for them, and re-layouts: 2.9 us -> 1.38 us
where the time goes in v2:
time: 67.8 us; the launch traced here: 67.6 us
  Pallas kernels  66.2 us (98%)
  local copies, waits for them, and re-layouts  1.38 us (2%)
    pallas_call x1, Pallas kernels, local(): pl.pallas_call(kernel, out_shape=jax.ShapeDtypeStruct((128, 128), BF), in...  66.2 us
    unnamed x1, local copies, waits for them, and re-layouts  1.38 us

profile of v2, /device:TPU:1, one launch (start us, length us, event | category | flops | bytes accessed | tf_op | source)
XLA Modules:
  0.0 67.6 jit_solution(3904460702518470692)
XLA Ops:
  0.0 66.2 %shard_map.82 = bf16[128,128]{1,0:T(8,128)(2,1)} custom-call(bf16[128,128]{1,0:T(8,128)(2,1)} %tok_ref.1, f32[3,1024]{1,0:T(4,128)} %gain_ref.1, bf16[3,64,128]{2,1,0:T(8,128)(2,1)} %wq_ref.1, bf16[3,64,128]{2,1,0:T(8,128)(2,1)} %wk_ref.1, bf16[3,64,128]{2,1,0:T(8,128)(2,1)} %wv_ref.1, bf16[3,64,128]{2,1,0:T(8,128)(2,1)} %bitcast.3, f32[6,8,16]{2,1,0:T(8,128)} %bitcast.4, ...), custom_call_target="tpu_custom_call" | custom-call | tf_op jit(solution)/shard_map/pallas_call | solution.py:298
  66.2 1.4 %copy.10 = bf16[128,128]{1,0:T(8,128)(2,1)} copy(bf16[128,128]{1,0:T(8,128)(2,1)} %shard_map.82) | data formatting | bytes 65536

commit v3 on v2

--- a/solution.py
+++ b/solution.py
@@ -1,3 +1,5 @@
+import math
+
 import jax
 import jax.numpy as jnp
 from jax import lax
@@ -14,38 +16,42 @@
 
 RING = (2, 1, 3)
 TP_PEERS = ((2, 0), (2, 1), (1, 0), (3, 0), (1, 1), (3, 1), (0, 1))
-Y_FIRST = 32
-N_COPIES = 160
+Y_FIRST = (32, 16)
+N_GROUPS = 48
+ALL_ROWS = 32768
 
 
 def kernel(
     tok_ref, gain_ref, wq_ref, wk_ref, wv_ref, wo_ref, bias_ref, docs_ref, out_ref,
-    W, WO, WL, G, A, KV, DOC, R, S, RX, SX, BM, PB, ssem, rsem, lsem,
+    W, WO, WL, G, A, KV, DOC, R, S, RX, SX, BM, PB, ALL, ssem, rsem, lsem,
 ):
     s = lax.axis_index("sp")
     t = lax.axis_index("tp")
     z, x = s // 4, s % 4
     y, c = t // 2, t % 2
-    sends = []
-
-    def rdma(src, dst, device):
-        sem = len(sends)
-        copy = pltpu.make_async_remote_copy(
-            src_ref=src,
-            dst_ref=dst,
-            send_sem=ssem.at[sem],
-            recv_sem=rsem.at[sem],
-            device_id=device,
-            device_id_type=MESH,
-        )
-        copy.start()
-        sends.append(copy)
-        return copy
-
-    def arrive(name, copies):
-        with jax.named_scope(name):
-            for copy in copies:
-                copy.wait_recv()
+    sent, groups = [], []
+
+    class Group:
+        def __init__(self, name, landing):
+            self.name, self.landing, self.sem = name, landing, rsem.at[len(groups)]
+            groups.append(self)
+
+        def send(self, src, dst, device, send_sem=None):
+            if send_sem is None:
+                send_sem = ssem.at[0]
+                sent.append(math.prod(src.shape) // 128)
+            pltpu.make_async_remote_copy(
+                src_ref=src,
+                dst_ref=dst,
+                send_sem=send_sem,
+                recv_sem=self.sem,
+                device_id=device,
+                device_id_type=MESH,
+            ).start()
+
+        def wait(self):
+            with jax.named_scope(self.name):
+                pltpu.make_async_copy(self.landing, self.landing, self.sem).wait()
 
     def x_peer(d):
         return {"sp": z * 4 + (x + d) % 4}
@@ -91,65 +97,121 @@
     with jax.named_scope("wait_barrier"):
         pl.semaphore_wait(barrier, len(greeted))
 
-    def block_one(ref, rows_a, rows_b):
-        along_x = [rdma(ref(z, x, rows_a), ref(z, x, rows_a), x_peer(d)) for d in RING]
-        along_z = [rdma(ref(z, x, rows_b), ref(z, x, rows_b), z_peer(d)) for d in RING]
-        return along_x + along_z
-
-    def block_two(ref, rows_a, rows_b):
-        every = slice(None)
-        then_z = [rdma(ref(z, every, rows_a), ref(z, every, rows_a), z_peer(d)) for d in RING]
-        then_x = [rdma(ref(every, x, rows_b), ref(every, x, rows_b), x_peer(d)) for d in RING]
-        return then_z + then_x
-
-    def halves(low, high):
-        mid = (low + high) // 2
-        return slice(low, mid), slice(mid, high)
-
-    class Gather:
+    every = slice(None)
+
+    class Plane:
         def __init__(self, name, ref, low, high):
-            self.name, self.ref, self.rows = name, ref, halves(low, high)
+            self.ref = ref
+            mid = (low + high) // 16 * 8
+            self.a, self.b = slice(low, mid), slice(mid, high)
+            rows = slice(low, high)
+            self.first = Group("p1_" + name, ref(0, slice(0, 3), rows))
+            self.second = Group("p2_" + name, ref(slice(0, 3), every, rows))
 
         def one(self):
-            self.first = block_one(self.ref, *self.rows)
+            for d in RING:
+                here = self.ref(z, x, self.a)
+                self.first.send(here, here, x_peer(d))
+                here = self.ref(z, x, self.b)
+                self.first.send(here, here, z_peer(d))
 
         def two(self):
-            arrive("p1_" + self.name, self.first)
-            self.second = block_two(self.ref, *self.rows)
+            self.first.wait()
+            for d in RING:
+                here = self.ref(z, every, self.a)
+                self.second.send(here, here, z_peer(d))
+                here = self.ref(every, x, self.b)
+                self.second.send(here, here, x_peer(d))
 
         def done(self):
-            arrive("p2_" + self.name, self.second)
+            self.second.wait()
+
+    class Prompt:
+        def __init__(self, name, ref):
+            self.ref = ref
+            self.a, self.b, self.all = slice(0, 32), slice(32, 64), slice(0, 64)
+            self.from_x = {d: Group(f"p1x{d}_{name}", ref(0, 0, self.all)) for d in (1, 3, 2)}
+            self.from_z = {d: Group(f"p1z{d}_{name}", ref(0, 0, self.all)) for d in (1, 3, 2)}
+            self.second = Group("p2_" + name, ref(slice(0, 3), slice(0, 3), self.all))
+
+        def one(self):
+            here = self.ref(z, x, self.all)
+            for d in (1, 3, 2):
+                self.from_x[d].send(here, here, x_peer(d))
+                self.from_z[d].send(here, here, z_peer(d))
+
+        def two(self):
+            for e in (1, 3, 2):
+                self.from_x[e].wait()
+                here = self.ref(z, (x - e + 4) % 4, self.a)
+                for d in (1, 3, 2):
+                    self.second.send(here, here, z_peer(d))
+                self.from_z[e].wait()
+                here = self.ref((z - e + 4) % 4, x, self.b)
+                for d in (1, 3, 2):
+                    self.second.send(here, here, x_peer(d))
+
+        def done(self):
+            self.second.wait()
 
     qkv = [
-        Gather(f"qkv{l}", lambda i, j, rows, l=l: W.at[l, :, i, j, rows], 0, 64)
+        (Plane if l else Prompt)(
+            f"qkv{l}", lambda i, j, rows, l=l: W.at[l, :, i, j, rows], *((0, 64) if l else ())
+        )
         for l in range(LAYERS)
     ]
     out_y = [
-        Gather(f"oy{l}", lambda i, j, rows, l=l: WO.at[l, :, i, j, rows], 0, Y_FIRST)
+        Plane(f"oy{l}", lambda i, j, rows, l=l: WO.at[l, :, i, j, rows], 0, Y_FIRST[l])
         for l in range(LAYERS - 1)
     ]
     out_p = [
-        Gather(f"op{l}", lambda i, j, rows, l=l: WO.at[l, y, i, j, rows], Y_FIRST, 64)
+        Plane(f"op{l}", lambda i, j, rows, l=l: WO.at[l, y, i, j, rows], Y_FIRST[l], 64)
         for l in range(LAYERS - 1)
     ]
-    out_last = Gather("ol", lambda i, j, rows: WL.at[i, j, rows], 0, 64)
+    out_last = Plane("ol", lambda i, j, rows: WL.at[i, j, rows], 0, 64)
+    cross_first = [
+        Group(f"cross{l}", WO.at[l, 0:3, 0, 0, 0 : Y_FIRST[l]]) for l in range(LAYERS - 1)
+    ]
+    cross_last = [
+        Group(f"cross_last{l}", WO.at[l, 0:3, :, :, Y_FIRST[l] : 64]) for l in range(LAYERS - 1)
+    ]
 
     def cross_y_first(l):
-        ref = WO.at[l, y, z, x, 0:Y_FIRST]
-        return [rdma(ref, ref, y_peer(d)) for d in RING]
+        ref = WO.at[l, y, z, x, 0 : Y_FIRST[l]]
+        for d in RING:
+            cross_first[l].send(ref, ref, y_peer(d))
 
     def cross_y_last(l):
-        ref = WO.at[l, y, :, :, Y_FIRST:64]
-        return [rdma(ref, ref, y_peer(d)) for d in RING]
-
-    gathers = [rdma(G.at[t], G.at[t], {"tp": tp_peer(dy, dc)}) for dy, dc in TP_PEERS]
-    doc_copies = [rdma(DOC.at[1], DOC.at[0], nxt), rdma(DOC.at[1], DOC.at[2], prv)]
+        out_p[l].done()
+        ref = WO.at[l, y, :, :, Y_FIRST[l] : 64]
+        for d in RING:
+            cross_last[l].send(ref, ref, y_peer(d))
+
+    tokens = Group("gather0", G.at[0:7])
+    attended_copies = [Group(f"gather{l + 1}", A.at[l, 0:3]) for l in range(LAYERS - 1)]
+    docs = Group("docs", DOC.at[0:2])
+    exchanges = [
+        [Group(f"exchange{l + 1}_{half}", RX.at[l, half]) for half in range(2)]
+        for l in range(LAYERS - 1)
+    ]
+    halos = [Group(f"halo{l}", KV.at[l, :, 0:224]) for l in range(LAYERS)]
+    reduces = Group("reduce", R)
+
     qkv[0].one()
-    crossed = [cross_y_first(l) for l in range(LAYERS - 1)]
-    crossed_last = [None, None]
+    for dy, dc in TP_PEERS:
+        tokens.send(G.at[t], G.at[t], {"tp": tp_peer(dy, dc)})
+    docs.send(DOC.at[1], DOC.at[0], nxt, ssem.at[1])
+    docs.send(DOC.at[1], DOC.at[2], prv, ssem.at[1])
+    cross_y_first(0)
     out_p[0].one()
-
-    arrive("docs", doc_copies)
+    cross_y_first(1)
+    out_p[1].one()
+    qkv[0].two()
+    out_p[0].two()
+    cross_first[0].wait()
+    out_y[0].one()
+
+    docs.wait()
     qi = lax.broadcasted_iota(jnp.int32, (128, 384), 0)
     kj = lax.broadcasted_iota(jnp.int32, (128, 384), 1)
     row_off = (kj >> 5) - (qi >> 5)
@@ -186,20 +248,16 @@
         mean = jnp.where(left, total0, total1) * (1.0 / 64)
         return values * lax.rsqrt(mean + EPS)
 
-    qkv[0].two()
-    arrive("cross0", crossed[0])
-    out_y[0].one()
-
     for l in range(LAYERS):
         if l == 0:
-            arrive("gather0", gathers)
+            tokens.wait()
             stream = [G[i].astype(F32) for i in range(8)]
         else:
-            arrive(f"gather{l}", gathers)
+            attended_copies[l - 1].wait()
             attended = jnp.concatenate([A[l - 1, i] for i in range(4)], axis=1)
             out_y[l - 1].done()
-            arrive(f"cross_last{l}", crossed_last[l - 1])
-            exchanges, parts = [], []
+            cross_last[l - 1].wait()
+            parts = []
             for half in range(2):
                 weight = jnp.concatenate(
                     [WO[l - 1, i, 2 * half : 2 * half + 2].reshape(512, 128) for i in range(4)], axis=1
@@ -208,11 +266,13 @@
                     attended, weight, (((1,), (1,)), ((), ())), preferred_element_type=F32
                 )
                 SX[l - 1, half] = part.astype(BF)
-                exchanges.append(rdma(SX.at[l - 1, half], RX.at[l - 1, half], partner))
+                exchanges[l - 1][half].send(SX.at[l - 1, half], RX.at[l - 1, half], partner)
                 parts.append(part)
+            if l == 1:
+                cross_y_last(1)
             stream = []
             for half in range(2):
-                arrive(f"exchange{l}_{half}", exchanges[half : half + 1])
+                exchanges[l - 1][half].wait()
                 whole = (parts[half] + RX[l - 1, half].astype(F32)).astype(BF).astype(F32)
                 stream += [whole[:, i * 128 : (i + 1) * 128] for i in range(4)]
         total = jnp.zeros((128, 1), F32)
@@ -227,29 +287,31 @@
             axis=1,
         )
         qkv[l].done()
+        if l == 0:
+            cross_y_last(0)
         key_raw = jnp.dot(normed, W[l, 1].reshape(1024, 128), preferred_element_type=F32)
         value_raw = jnp.dot(normed, W[l, 2].reshape(1024, 128), preferred_element_type=F32)
         KV[l, 0, 128:256] = head_norm(key_raw).astype(BF)
         KV[l, 1, 128:256] = value_raw.astype(BF)
-        halos = [
-            rdma(KV.at[l, :, 128:256], KV.at[l, :, 0:128], nxt),
-            rdma(KV.at[l, :, 128:224], KV.at[l, :, 256:352], prv),
-        ]
+        halos[l].send(KV.at[l, :, 128:256], KV.at[l, :, 0:128], nxt)
+        halos[l].send(KV.at[l, :, 128:224], KV.at[l, :, 256:352], prv)
         if l == 0:
             qkv[1].one()
-            out_p[0].two()
             out_y[0].two()
+            out_p[1].two()
+            cross_first[1].wait()
+            out_y[1].one()
         elif l == 1:
-            qkv[2].one()
-            out_p[1].two()
             out_y[1].two()
+            qkv[2].two()
+            out_last.one()
         query = head_norm(
             jnp.dot(normed, W[l, 0].reshape(1024, 128), preferred_element_type=F32)
         ).astype(BF)
         query = query * jnp.asarray(0.125, BF)
         zero = jnp.zeros_like(query)
         query = jnp.concatenate([jnp.where(left, query, zero), jnp.where(left, zero, query)], axis=0)
-        arrive(f"halo{l}", halos)
+        halos[l].wait()
         scores = lax.dot_general(
             query, KV[l, 0], (((1,), (1,)), ((), ())), preferred_element_type=F32
         ) + BM[l]
@@ -259,15 +321,11 @@
         heads = jnp.where(left, mixed[:128], mixed[128:]).astype(BF)
         if l < LAYERS - 1:
             A[l, y] = heads
-            gathers = [rdma(A.at[l, y], A.at[l, y], y_peer(d)) for d in RING]
-            qkv[l + 1].two()
-            out_p[l].done()
-            crossed_last[l] = cross_y_last(l)
+            for d in RING:
+                attended_copies[l].send(A.at[l, y], A.at[l, y], y_peer(d))
             if l == 0:
-                out_p[1].one()
-                arrive("cross1", crossed[1])
-                out_y[1].one()
-                out_last.one()
+                qkv[1].two()
+                qkv[2].one()
             else:
                 out_last.two()
             continue
@@ -277,19 +335,19 @@
         ).astype(BF)
         for i in range(8):
             S[i] = partial[:, i * 128 : (i + 1) * 128]
-        reduces = []
         for i, (dy, dc) in enumerate(TP_PEERS):
             peer = tp_peer(dy, dc)
-            reduces.append(rdma(S.at[peer], R.at[i], {"tp": peer}))
+            reduces.send(S.at[peer], R.at[i], {"tp": peer})
         result = S[t].astype(F32)
-        arrive("reduce", reduces)
+        reduces.wait()
         for i in range(7):
             result += R[i].astype(F32)
         out_ref[...] = result.astype(BF)
 
     with jax.named_scope("wait_sends"):
-        for copy in sends:
-            copy.wait_send()
+        pltpu.make_async_copy(DOC.at[0:2], DOC.at[0:2], ssem.at[1]).wait()
+        everything = ALL.at[0 : sum(sent)]
+        pltpu.make_async_copy(everything, everything, ssem.at[0]).wait()
 
 
 def local(tokens, norm_gain, w_query, w_key, w_value, w_out, offset_bias, documents):
@@ -314,8 +372,9 @@
             pltpu.VMEM((LAYERS - 1, 2, 128, 512), BF),
             pltpu.VMEM((LAYERS, 256, 384), F32),
             pltpu.VMEM((6, 512), F32),
-            pltpu.SemaphoreType.DMA((N_COPIES,)),
-            pltpu.SemaphoreType.DMA((N_COPIES,)),
+            pltpu.VMEM((ALL_ROWS, 128), BF),
+            pltpu.SemaphoreType.DMA((2,)),
+            pltpu.SemaphoreType.DMA((N_GROUPS,)),
             pltpu.SemaphoreType.DMA((7,)),
         ],
         compiler_params=pltpu.CompilerParams(collective_id=0, has_side_effects=True),

time: 67.8 us -> 59.1 us (0.87)
  Pallas kernels: 66.2 us -> 57.4 us
    pallas_call x1, Pallas kernels: 66.2 us -> 57.4 us  [local(): pl.pallas_call(kernel, out_shape=jax.ShapeDtypeStruct((128, 128), BF), in...]
where the time goes in v3:
time: 59.1 us; the launch traced here: 58.8 us
  Pallas kernels  57.4 us (97%)
  local copies, waits for them, and re-layouts  1.38 us (2%)
    pallas_call x1, Pallas kernels, local(): pl.pallas_call(kernel, out_shape=jax.ShapeDtypeStruct((128, 128), BF), in...  57.4 us
    unnamed x1, local copies, waits for them, and re-layouts  1.38 us

profile of v3, /device:TPU:1, one launch (start us, length us, event | category | flops | bytes accessed | tf_op | source)
XLA Modules:
  0.0 58.8 jit_solution(17857980399664844994)
XLA Ops:
  0.0 57.4 %shard_map.82 = bf16[128,128]{1,0:T(8,128)(2,1)} custom-call(bf16[128,128]{1,0:T(8,128)(2,1)} %tok_ref.1, f32[3,1024]{1,0:T(4,128)} %gain_ref.1, bf16[3,64,128]{2,1,0:T(8,128)(2,1)} %wq_ref.1, bf16[3,64,128]{2,1,0:T(8,128)(2,1)} %wk_ref.1, bf16[3,64,128]{2,1,0:T(8,128)(2,1)} %wv_ref.1, bf16[3,64,128]{2,1,0:T(8,128)(2,1)} %bitcast.3, f32[6,8,16]{2,1,0:T(8,128)} %bitcast.4, ...), custom_call_target="tpu_custom_call" | custom-call | tf_op jit(solution)/shard_map/pallas_call | solution.py:356
  57.4 1.4 %copy.10 = bf16[128,128]{1,0:T(8,128)(2,1)} copy(bf16[128,128]{1,0:T(8,128)(2,1)} %shard_map.82) | data formatting | bytes 65536

commit v4 on v3

--- a/solution.py
+++ b/solution.py
@@ -16,14 +16,14 @@
 
 RING = (2, 1, 3)
 TP_PEERS = ((2, 0), (2, 1), (1, 0), (3, 0), (1, 1), (3, 1), (0, 1))
-Y_FIRST = (32, 16)
-N_GROUPS = 48
+Y_FIRST = (32, 32)
+N_GROUPS = 64
 ALL_ROWS = 32768
 
 
 def kernel(
     tok_ref, gain_ref, wq_ref, wk_ref, wv_ref, wo_ref, bias_ref, docs_ref, out_ref,
-    W, WO, WL, G, A, KV, DOC, R, S, RX, SX, BM, PB, ALL, ssem, rsem, lsem,
+    GAIN, BIAS, W, WO, WL, G, A, KV, DOC, R, S, RX, SX, PART, BM, PB, ALL, ssem, rsem, lsem,
 ):
     s = lax.axis_index("sp")
     t = lax.axis_index("tp")
@@ -71,11 +71,13 @@
     local = [
         pltpu.make_async_copy(tok_ref, G.at[t], lsem.at[0]),
         pltpu.make_async_copy(docs_ref, DOC.at[1], lsem.at[1]),
-        pltpu.make_async_copy(wq_ref, W.at[:, 0, z, x], lsem.at[2]),
-        pltpu.make_async_copy(wk_ref, W.at[:, 1, z, x], lsem.at[3]),
-        pltpu.make_async_copy(wv_ref, W.at[:, 2, z, x], lsem.at[4]),
+        pltpu.make_async_copy(wq_ref, W.at[:, 2, z, x], lsem.at[2]),
+        pltpu.make_async_copy(wk_ref, W.at[:, 0, z, x], lsem.at[3]),
+        pltpu.make_async_copy(wv_ref, W.at[:, 1, z, x], lsem.at[4]),
         pltpu.make_async_copy(wo_ref.at[0:2], WO.at[:, y, z, x], lsem.at[5]),
         pltpu.make_async_copy(wo_ref.at[2], WL.at[z, x], lsem.at[6]),
+        pltpu.make_async_copy(gain_ref, GAIN, lsem.at[7]),
+        pltpu.make_async_copy(bias_ref, BIAS, lsem.at[8]),
     ]
     with jax.named_scope("init"):
         for copy in local:
@@ -154,10 +156,14 @@
         def done(self):
             self.second.wait()
 
-    qkv = [
+    kv = [
         (Plane if l else Prompt)(
-            f"qkv{l}", lambda i, j, rows, l=l: W.at[l, :, i, j, rows], *((0, 64) if l else ())
+            f"kv{l}", lambda i, j, rows, l=l: W.at[l, 0:2, i, j, rows], *((0, 64) if l else ())
         )
+        for l in range(LAYERS)
+    ]
+    wq = [
+        Plane(f"q{l}", lambda i, j, rows, l=l: W.at[l, 2, i, j, rows], 0, 64)
         for l in range(LAYERS)
     ]
     out_y = [
@@ -188,7 +194,9 @@
             cross_last[l].send(ref, ref, y_peer(d))
 
     tokens = Group("gather0", G.at[0:7])
-    attended_copies = [Group(f"gather{l + 1}", A.at[l, 0:3]) for l in range(LAYERS - 1)]
+    attended_copies = [
+        {d: Group(f"gather{l + 1}_{d}", A.at[l, 0]) for d in RING} for l in range(LAYERS - 1)
+    ]
     docs = Group("docs", DOC.at[0:2])
     exchanges = [
         [Group(f"exchange{l + 1}_{half}", RX.at[l, half]) for half in range(2)]
@@ -197,7 +205,7 @@
     halos = [Group(f"halo{l}", KV.at[l, :, 0:224]) for l in range(LAYERS)]
     reduces = Group("reduce", R)
 
-    qkv[0].one()
+    kv[0].one()
     for dy, dc in TP_PEERS:
         tokens.send(G.at[t], G.at[t], {"tp": tp_peer(dy, dc)})
     docs.send(DOC.at[1], DOC.at[0], nxt, ssem.at[1])
@@ -205,11 +213,12 @@
     cross_y_first(0)
     out_p[0].one()
     cross_y_first(1)
-    out_p[1].one()
-    qkv[0].two()
+    kv[0].two()
+    wq[0].one()
     out_p[0].two()
     cross_first[0].wait()
     out_y[0].one()
+    out_p[1].one()
 
     docs.wait()
     qi = lax.broadcasted_iota(jnp.int32, (128, 384), 0)
@@ -229,7 +238,7 @@
     )
     lines = jnp.zeros((6, 512), F32)
     for a in range(8):
-        PB[:, 0:16] = bias_ref[:, a, :]
+        PB[:, 0:16] = BIAS[:, a, :]
         lines += pltpu.roll(PB[...], 119 + 32 * a, 1)
     for l in range(LAYERS):
         for h in range(2):
@@ -253,18 +262,28 @@
             tokens.wait()
             stream = [G[i].astype(F32) for i in range(8)]
         else:
-            attended_copies[l - 1].wait()
-            attended = jnp.concatenate([A[l - 1, i] for i in range(4)], axis=1)
             out_y[l - 1].done()
             cross_last[l - 1].wait()
+
+            def project(slabs, half):
+                weight = jnp.concatenate(
+                    [WO[l - 1, i, 2 * half : 2 * half + 2].reshape(512, 128) for i in slabs], axis=1
+                )
+                some = jnp.concatenate([A[l - 1, i] for i in slabs], axis=1)
+                return lax.dot_general(
+                    some, weight, (((1,), (1,)), ((), ())), preferred_element_type=F32
+                )
+
+            attended_copies[l - 1][1].wait()
+            early = (y, (y + 3) % 4)
+            for half in range(2):
+                PART[half] = project(early, half)
+            attended_copies[l - 1][3].wait()
+            attended_copies[l - 1][2].wait()
+            late = ((y + 1) % 4, (y + 2) % 4)
             parts = []
             for half in range(2):
-                weight = jnp.concatenate(
-                    [WO[l - 1, i, 2 * half : 2 * half + 2].reshape(512, 128) for i in range(4)], axis=1
-                )
-                part = lax.dot_general(
-                    attended, weight, (((1,), (1,)), ((), ())), preferred_element_type=F32
-                )
+                part = PART[half] + project(late, half)
                 SX[l - 1, half] = part.astype(BF)
                 exchanges[l - 1][half].send(SX.at[l - 1, half], RX.at[l - 1, half], partner)
                 parts.append(part)
@@ -281,32 +300,34 @@
         scale = lax.rsqrt(total * (1.0 / 1024) + EPS)
         normed = jnp.concatenate(
             [
-                (part * scale * gain_ref[l : l + 1, i * 128 : (i + 1) * 128]).astype(BF)
+                (part * scale * GAIN[l : l + 1, i * 128 : (i + 1) * 128]).astype(BF)
                 for i, part in enumerate(stream)
             ],
             axis=1,
         )
-        qkv[l].done()
-        if l == 0:
-            cross_y_last(0)
-        key_raw = jnp.dot(normed, W[l, 1].reshape(1024, 128), preferred_element_type=F32)
-        value_raw = jnp.dot(normed, W[l, 2].reshape(1024, 128), preferred_element_type=F32)
+        kv[l].done()
+        key_raw = jnp.dot(normed, W[l, 0].reshape(1024, 128), preferred_element_type=F32)
+        value_raw = jnp.dot(normed, W[l, 1].reshape(1024, 128), preferred_element_type=F32)
         KV[l, 0, 128:256] = head_norm(key_raw).astype(BF)
         KV[l, 1, 128:256] = value_raw.astype(BF)
         halos[l].send(KV.at[l, :, 128:256], KV.at[l, :, 0:128], nxt)
         halos[l].send(KV.at[l, :, 128:224], KV.at[l, :, 256:352], prv)
         if l == 0:
-            qkv[1].one()
+            wq[0].two()
+            cross_y_last(0)
+            kv[1].one()
+            wq[1].one()
             out_y[0].two()
             out_p[1].two()
-            cross_first[1].wait()
-            out_y[1].one()
         elif l == 1:
             out_y[1].two()
-            qkv[2].two()
-            out_last.one()
+            kv[2].two()
+            wq[2].two()
+        else:
+            out_last.two()
+        wq[l].done()
         query = head_norm(
-            jnp.dot(normed, W[l, 0].reshape(1024, 128), preferred_element_type=F32)
+            jnp.dot(normed, W[l, 2].reshape(1024, 128), preferred_element_type=F32)
         ).astype(BF)
         query = query * jnp.asarray(0.125, BF)
         zero = jnp.zeros_like(query)
@@ -322,23 +343,29 @@
         if l < LAYERS - 1:
             A[l, y] = heads
             for d in RING:
-                attended_copies[l].send(A.at[l, y], A.at[l, y], y_peer(d))
+                attended_copies[l][d].send(A.at[l, y], A.at[l, y], y_peer(d))
             if l == 0:
-                qkv[1].two()
-                qkv[2].one()
-            else:
-                out_last.two()
+                kv[1].two()
+                wq[1].two()
+                cross_first[1].wait()
+                kv[2].one()
+                out_y[1].one()
+                wq[2].one()
+                out_last.one()
             continue
         out_last.done()
-        partial = lax.dot_general(
-            heads, WL[...].reshape(1024, 128), (((1,), (1,)), ((), ())), preferred_element_type=F32
-        ).astype(BF)
-        for i in range(8):
-            S[i] = partial[:, i * 128 : (i + 1) * 128]
+
+        def project_last(to):
+            weight = WL[to // 2, pl.ds(to % 2 * 2, 2)].reshape(128, 128)
+            return lax.dot_general(
+                heads, weight, (((1,), (1,)), ((), ())), preferred_element_type=F32
+            )
+
         for i, (dy, dc) in enumerate(TP_PEERS):
             peer = tp_peer(dy, dc)
-            reduces.send(S.at[peer], R.at[i], {"tp": peer})
-        result = S[t].astype(F32)
+            S[i] = project_last(peer).astype(BF)
+            reduces.send(S.at[i], R.at[i], {"tp": peer})
+        result = project_last(t)
         reduces.wait()
         for i in range(7):
             result += R[i].astype(F32)
@@ -356,9 +383,11 @@
     return pl.pallas_call(
         kernel,
         out_shape=jax.ShapeDtypeStruct((128, 128), BF),
-        in_specs=[hbm, vmem, hbm, hbm, hbm, hbm, vmem, hbm],
+        in_specs=[hbm] * 8,
         out_specs=vmem,
         scratch_shapes=[
+            pltpu.VMEM((LAYERS, 1024), F32),
+            pltpu.VMEM((2 * LAYERS, 8, 16), F32),
             pltpu.VMEM((LAYERS, 3, 4, 4, 64, 128), BF),
             pltpu.VMEM((LAYERS - 1, 4, 4, 4, 64, 128), BF),
             pltpu.VMEM((4, 4, 64, 128), BF),
@@ -367,15 +396,16 @@
             pltpu.VMEM((LAYERS, 2, 384, 128), BF),
             pltpu.VMEM((3, 1, 128), jnp.int32),
             pltpu.VMEM((7, 128, 128), BF),
-            pltpu.VMEM((8, 128, 128), BF),
+            pltpu.VMEM((7, 128, 128), BF),
             pltpu.VMEM((LAYERS - 1, 2, 128, 512), BF),
             pltpu.VMEM((LAYERS - 1, 2, 128, 512), BF),
+            pltpu.VMEM((2, 128, 512), F32),
             pltpu.VMEM((LAYERS, 256, 384), F32),
             pltpu.VMEM((6, 512), F32),
             pltpu.VMEM((ALL_ROWS, 128), BF),
             pltpu.SemaphoreType.DMA((2,)),
             pltpu.SemaphoreType.DMA((N_GROUPS,)),
-            pltpu.SemaphoreType.DMA((7,)),
+            pltpu.SemaphoreType.DMA((9,)),
         ],
         compiler_params=pltpu.CompilerParams(collective_id=0, has_side_effects=True),
     )(

time: 59.1 us -> 56.2 us (0.951)
  Pallas kernels: 57.4 us -> 54.6 us
    pallas_call x1, Pallas kernels: 57.4 us -> 54.6 us  [local(): pl.pallas_call(kernel, out_shape=jax.ShapeDtypeStruct((128, 128), BF), in...]
where the time goes in v4:
time: 56.2 us; the launch traced here: 56 us
  Pallas kernels  54.6 us (97%)
  local copies, waits for them, and re-layouts  1.38 us (2%)
    pallas_call x1, Pallas kernels, local(): pl.pallas_call(kernel, out_shape=jax.ShapeDtypeStruct((128, 128), BF), in...  54.6 us
    unnamed x1, local copies, waits for them, and re-layouts  1.38 us

profile of v4, /device:TPU:1, one launch (start us, length us, event | category | flops | bytes accessed | tf_op | source)
XLA Modules:
  0.0 56.0 jit_solution(1290657191518679337)
XLA Ops:
  0.0 54.6 %shard_map.82 = bf16[128,128]{1,0:T(8,128)(2,1)} custom-call(bf16[128,128]{1,0:T(8,128)(2,1)} %tok_ref.1, f32[3,1024]{1,0:T(4,128)} %gain_ref.1, bf16[3,64,128]{2,1,0:T(8,128)(2,1)} %wq_ref.1, bf16[3,64,128]{2,1,0:T(8,128)(2,1)} %wk_ref.1, bf16[3,64,128]{2,1,0:T(8,128)(2,1)} %wv_ref.1, bf16[3,64,128]{2,1,0:T(8,128)(2,1)} %bitcast.3, f32[6,8,16]{2,1,0:T(8,128)} %bitcast.4, ...), custom_call_target="tpu_custom_call" | custom-call | tf_op jit(solution)/shard_map/pallas_call | solution.py:383
  54.6 1.4 %copy.10 = bf16[128,128]{1,0:T(8,128)(2,1)} copy(bf16[128,128]{1,0:T(8,128)(2,1)} %shard_map.82) | data formatting | bytes 65536

commit v5 on v4

--- a/solution.py
+++ b/solution.py
@@ -218,7 +218,6 @@
     out_p[0].two()
     cross_first[0].wait()
     out_y[0].one()
-    out_p[1].one()
 
     docs.wait()
     qi = lax.broadcasted_iota(jnp.int32, (128, 384), 0)
@@ -294,9 +293,10 @@
                 exchanges[l - 1][half].wait()
                 whole = (parts[half] + RX[l - 1, half].astype(F32)).astype(BF).astype(F32)
                 stream += [whole[:, i * 128 : (i + 1) * 128] for i in range(4)]
-        total = jnp.zeros((128, 1), F32)
-        for part in stream:
-            total += jnp.sum(part * part, axis=1, keepdims=True)
+        squares = stream[0] * stream[0]
+        for part in stream[1:]:
+            squares += part * part
+        total = jnp.sum(squares, axis=1, keepdims=True)
         scale = lax.rsqrt(total * (1.0 / 1024) + EPS)
         normed = jnp.concatenate(
             [
@@ -306,25 +306,26 @@
             axis=1,
         )
         kv[l].done()
+        KV[l, 1, 128:256] = jnp.dot(
+            normed, W[l, 1].reshape(1024, 128), preferred_element_type=F32
+        ).astype(BF)
+        halos[l].send(KV.at[l, 1, 128:256], KV.at[l, 1, 0:128], nxt)
+        halos[l].send(KV.at[l, 1, 128:224], KV.at[l, 1, 256:352], prv)
         key_raw = jnp.dot(normed, W[l, 0].reshape(1024, 128), preferred_element_type=F32)
-        value_raw = jnp.dot(normed, W[l, 1].reshape(1024, 128), preferred_element_type=F32)
         KV[l, 0, 128:256] = head_norm(key_raw).astype(BF)
-        KV[l, 1, 128:256] = value_raw.astype(BF)
-        halos[l].send(KV.at[l, :, 128:256], KV.at[l, :, 0:128], nxt)
-        halos[l].send(KV.at[l, :, 128:224], KV.at[l, :, 256:352], prv)
+        halos[l].send(KV.at[l, 0, 128:256], KV.at[l, 0, 0:128], nxt)
+        halos[l].send(KV.at[l, 0, 128:224], KV.at[l, 0, 256:352], prv)
         if l == 0:
             wq[0].two()
+            out_p[1].one()
             cross_y_last(0)
             kv[1].one()
             wq[1].one()
             out_y[0].two()
-            out_p[1].two()
         elif l == 1:
             out_y[1].two()
             kv[2].two()
             wq[2].two()
-        else:
-            out_last.two()
         wq[l].done()
         query = head_norm(
             jnp.dot(normed, W[l, 2].reshape(1024, 128), preferred_element_type=F32)
@@ -336,7 +337,7 @@
         scores = lax.dot_general(
             query, KV[l, 0], (((1,), (1,)), ((), ())), preferred_element_type=F32
         ) + BM[l]
-        probs = jnp.exp(scores - jnp.max(scores, axis=1, keepdims=True))
+        probs = jnp.exp(scores)
         norm = jnp.sum(probs, axis=1, keepdims=True)
         mixed = jnp.dot(probs.astype(BF), KV[l, 1], preferred_element_type=F32) / norm
         heads = jnp.where(left, mixed[:128], mixed[128:]).astype(BF)
@@ -345,6 +346,7 @@
             for d in RING:
                 attended_copies[l][d].send(A.at[l, y], A.at[l, y], y_peer(d))
             if l == 0:
+                out_p[1].two()
                 kv[1].two()
                 wq[1].two()
                 cross_first[1].wait()
@@ -352,6 +354,8 @@
                 out_y[1].one()
                 wq[2].one()
                 out_last.one()
+            else:
+                out_last.two()
             continue
         out_last.done()
 

time: 56.2 us -> 56 us (level)
  no operation moved by 1% of the time
where the time goes in v5:
time: 56 us; the launch traced here: 55.7 us
  Pallas kernels  54.4 us (97%)
  local copies, waits for them, and re-layouts  1.38 us (2%)
    pallas_call x1, Pallas kernels, local(): pl.pallas_call(kernel, out_shape=jax.ShapeDtypeStruct((128, 128), BF), in...  54.4 us
    unnamed x1, local copies, waits for them, and re-layouts  1.38 us

profile of v5, /device:TPU:1, one launch (start us, length us, event | category | flops | bytes accessed | tf_op | source)
XLA Modules:
  0.0 55.7 jit_solution(4839512346207240096)
XLA Ops:
  0.0 54.4 %shard_map.82 = bf16[128,128]{1,0:T(8,128)(2,1)} custom-call(bf16[128,128]{1,0:T(8,128)(2,1)} %tok_ref.1, f32[3,1024]{1,0:T(4,128)} %gain_ref.1, bf16[3,64,128]{2,1,0:T(8,128)(2,1)} %wq_ref.1, bf16[3,64,128]{2,1,0:T(8,128)(2,1)} %wk_ref.1, bf16[3,64,128]{2,1,0:T(8,128)(2,1)} %wv_ref.1, bf16[3,64,128]{2,1,0:T(8,128)(2,1)} %bitcast.3, f32[6,8,16]{2,1,0:T(8,128)} %bitcast.4, ...), custom_call_target="tpu_custom_call" | custom-call | tf_op jit(solution)/shard_map/pallas_call | solution.py:387
  54.4 1.4 %copy.10 = bf16[128,128]{1,0:T(8,128)(2,1)} copy(bf16[128,128]{1,0:T(8,128)(2,1)} %shard_map.82) | data formatting | bytes 65536

commit v6 on v5

--- a/solution.py
+++ b/solution.py
@@ -16,14 +16,14 @@
 
 RING = (2, 1, 3)
 TP_PEERS = ((2, 0), (2, 1), (1, 0), (3, 0), (1, 1), (3, 1), (0, 1))
-Y_FIRST = (32, 32)
+Y_FIRST = (32, 48)
 N_GROUPS = 64
 ALL_ROWS = 32768
 
 
 def kernel(
     tok_ref, gain_ref, wq_ref, wk_ref, wv_ref, wo_ref, bias_ref, docs_ref, out_ref,
-    GAIN, BIAS, W, WO, WL, G, A, KV, DOC, R, S, RX, SX, PART, BM, PB, ALL, ssem, rsem, lsem,
+    GAIN, BIAS, W, WO, WL, G, A, KV, DOC, R, S, WP, HS, HR, RX, SX, PART, BM, PB, ALL, ssem, rsem, lsem,
 ):
     s = lax.axis_index("sp")
     t = lax.axis_index("tp")
@@ -146,11 +146,11 @@
             for e in (1, 3, 2):
                 self.from_x[e].wait()
                 here = self.ref(z, (x - e + 4) % 4, self.a)
-                for d in (1, 3, 2):
+                for d in RING:
                     self.second.send(here, here, z_peer(d))
                 self.from_z[e].wait()
                 here = self.ref((z - e + 4) % 4, x, self.b)
-                for d in (1, 3, 2):
+                for d in RING:
                     self.second.send(here, here, x_peer(d))
 
         def done(self):
@@ -204,6 +204,8 @@
     ]
     halos = [Group(f"halo{l}", KV.at[l, :, 0:224]) for l in range(LAYERS)]
     reduces = Group("reduce", R)
+    last_weights = Group("last_weights", WP)
+    swap = Group("swap", HR)
 
     kv[0].one()
     for dy, dc in TP_PEERS:
@@ -326,6 +328,9 @@
             out_y[1].two()
             kv[2].two()
             wq[2].two()
+        else:
+            out_last.done()
+            last_weights.send(WL.at[:, pl.ds(2 * (1 - c), 2)], WP, partner)
         wq[l].done()
         query = head_norm(
             jnp.dot(normed, W[l, 2].reshape(1024, 128), preferred_element_type=F32)
@@ -357,21 +362,25 @@
             else:
                 out_last.two()
             continue
-        out_last.done()
-
-        def project_last(to):
-            weight = WL[to // 2, pl.ds(to % 2 * 2, 2)].reshape(128, 128)
+        HS[...] = heads
+        swap.send(HS, HR, partner)
+
+        def project_last(some, weight):
             return lax.dot_general(
-                heads, weight, (((1,), (1,)), ((), ())), preferred_element_type=F32
+                some, weight.reshape(512, 128), (((1,), (1,)), ((), ())), preferred_element_type=F32
             )
 
-        for i, (dy, dc) in enumerate(TP_PEERS):
-            peer = tp_peer(dy, dc)
-            S[i] = project_last(peer).astype(BF)
-            reduces.send(S.at[i], R.at[i], {"tp": peer})
-        result = project_last(t)
+        own = project_last(heads, WL[:, pl.ds(2 * c, 2)])
+        last_weights.wait()
+        swap.wait()
+        own += project_last(HR[...], WP[...])
+        for i in range(4):
+            S[i] = own[:, i * 128 : (i + 1) * 128].astype(BF)
+        for i, d in enumerate(RING):
+            reduces.send(S.at[(y + d) % 4], R.at[i], y_peer(d))
+        result = S[y].astype(F32)
         reduces.wait()
-        for i in range(7):
+        for i in range(3):
             result += R[i].astype(F32)
         out_ref[...] = result.astype(BF)
 
@@ -399,8 +408,11 @@
             pltpu.VMEM((LAYERS - 1, 4, 128, 128), BF),
             pltpu.VMEM((LAYERS, 2, 384, 128), BF),
             pltpu.VMEM((3, 1, 128), jnp.int32),
-            pltpu.VMEM((7, 128, 128), BF),
-            pltpu.VMEM((7, 128, 128), BF),
+            pltpu.VMEM((3, 128, 128), BF),
+            pltpu.VMEM((4, 128, 128), BF),
+            pltpu.VMEM((4, 2, 64, 128), BF),
+            pltpu.VMEM((128, 128), BF),
+            pltpu.VMEM((128, 128), BF),
             pltpu.VMEM((LAYERS - 1, 2, 128, 512), BF),
             pltpu.VMEM((LAYERS - 1, 2, 128, 512), BF),
             pltpu.VMEM((2, 128, 512), F32),

time: 56 us -> 55.3 us (0.987)
  Pallas kernels: 54.4 us -> 53.6 us
    pallas_call x1, Pallas kernels: 54.4 us -> 53.6 us  [local(): pl.pallas_call(kernel, out_shape=jax.ShapeDtypeStruct((128, 128), BF), in...]
where the time goes in v6:
time: 55.3 us; the launch traced here: 55 us
  Pallas kernels  53.6 us (97%)
  local copies, waits for them, and re-layouts  1.38 us (2%)
    pallas_call x1, Pallas kernels, local(): pl.pallas_call(kernel, out_shape=jax.ShapeDtypeStruct((128, 128), BF), in...  53.6 us
    unnamed x1, local copies, waits for them, and re-layouts  1.38 us

profile of v6, /device:TPU:1, one launch (start us, length us, event | category | flops | bytes accessed | tf_op | source)
XLA Modules:
  0.0 55.0 jit_solution(6624003617690755761)
XLA Ops:
  0.0 53.6 %shard_map.82 = bf16[128,128]{1,0:T(8,128)(2,1)} custom-call(bf16[128,128]{1,0:T(8,128)(2,1)} %tok_ref.1, f32[3,1024]{1,0:T(4,128)} %gain_ref.1, bf16[3,64,128]{2,1,0:T(8,128)(2,1)} %wq_ref.1, bf16[3,64,128]{2,1,0:T(8,128)(2,1)} %wk_ref.1, bf16[3,64,128]{2,1,0:T(8,128)(2,1)} %wv_ref.1, bf16[3,64,128]{2,1,0:T(8,128)(2,1)} %bitcast.3, f32[6,8,16]{2,1,0:T(8,128)} %bitcast.4, ...), custom_call_target="tpu_custom_call" | custom-call | tf_op jit(solution)/shard_map/pallas_call | solution.py:396
  53.7 1.4 %copy.10 = bf16[128,128]{1,0:T(8,128)(2,1)} copy(bf16[128,128]{1,0:T(8,128)(2,1)} %shard_map.82) | data formatting | bytes 65536

commit v7 on v6

--- a/solution.py
+++ b/solution.py
@@ -16,7 +16,7 @@
 
 RING = (2, 1, 3)
 TP_PEERS = ((2, 0), (2, 1), (1, 0), (3, 0), (1, 1), (3, 1), (0, 1))
-Y_FIRST = (32, 48)
+Y_FIRST = (32, 32)
 N_GROUPS = 64
 ALL_ROWS = 32768
 
@@ -128,6 +128,32 @@
         def done(self):
             self.second.wait()
 
+    class Relay(Plane):
+        def __init__(self, name, ref, low, high):
+            super().__init__(name, ref, low, high)
+            rows = slice(low, high)
+            self.near = Group("near_" + name, ref(slice(0, 2), every, rows))
+            self.far = Group("far_" + name, ref(0, every, rows))
+
+        def two(self):
+            self.first.wait()
+            for d in (1, 3):
+                here = self.ref(z, every, self.a)
+                self.near.send(here, here, z_peer(d))
+                here = self.ref(every, x, self.b)
+                self.near.send(here, here, x_peer(d))
+
+        def three(self):
+            self.near.wait()
+            for d, part in ((1, slice(0, 2)), (3, slice(2, 4))):
+                here = self.ref((z - d + 4) % 4, part, self.a)
+                self.far.send(here, here, z_peer(d))
+                here = self.ref(part, (x - d + 4) % 4, self.b)
+                self.far.send(here, here, x_peer(d))
+
+        def done(self):
+            self.far.wait()
+
     class Prompt:
         def __init__(self, name, ref):
             self.ref = ref
@@ -157,13 +183,13 @@
             self.second.wait()
 
     kv = [
-        (Plane if l else Prompt)(
+        (Relay if l == 1 else Plane if l else Prompt)(
             f"kv{l}", lambda i, j, rows, l=l: W.at[l, 0:2, i, j, rows], *((0, 64) if l else ())
         )
         for l in range(LAYERS)
     ]
     wq = [
-        Plane(f"q{l}", lambda i, j, rows, l=l: W.at[l, 2, i, j, rows], 0, 64)
+        (Relay if l == 1 else Plane)(f"q{l}", lambda i, j, rows, l=l: W.at[l, 2, i, j, rows], 0, 64)
         for l in range(LAYERS)
     ]
     out_y = [
@@ -214,12 +240,16 @@
     docs.send(DOC.at[1], DOC.at[2], prv, ssem.at[1])
     cross_y_first(0)
     out_p[0].one()
+    wq[0].one()
     cross_y_first(1)
     kv[0].two()
-    wq[0].one()
     out_p[0].two()
+    wq[0].two()
     cross_first[0].wait()
     out_y[0].one()
+    out_p[1].one()
+    kv[1].one()
+    wq[1].one()
 
     docs.wait()
     qi = lax.broadcasted_iota(jnp.int32, (128, 384), 0)
@@ -318,12 +348,11 @@
         halos[l].send(KV.at[l, 0, 128:256], KV.at[l, 0, 0:128], nxt)
         halos[l].send(KV.at[l, 0, 128:224], KV.at[l, 0, 256:352], prv)
         if l == 0:
-            wq[0].two()
-            out_p[1].one()
             cross_y_last(0)
-            kv[1].one()
-            wq[1].one()
             out_y[0].two()
+            out_p[1].two()
+            kv[1].two()
+            wq[1].two()
         elif l == 1:
             out_y[1].two()
             kv[2].two()
@@ -351,9 +380,8 @@
             for d in RING:
                 attended_copies[l][d].send(A.at[l, y], A.at[l, y], y_peer(d))
             if l == 0:
-                out_p[1].two()
-                kv[1].two()
-                wq[1].two()
+                kv[1].three()
+                wq[1].three()
                 cross_first[1].wait()
                 kv[2].one()
                 out_y[1].one()

time: 55.3 us -> 53.4 us (0.966)
  Pallas kernels: 53.6 us -> 51.7 us
    pallas_call x1, Pallas kernels: 53.6 us -> 51.7 us  [local(): pl.pallas_call(kernel, out_shape=jax.ShapeDtypeStruct((128, 128), BF), in...]
where the time goes in v7:
time: 53.4 us; the launch traced here: 53.1 us
  Pallas kernels  51.7 us (97%)
  local copies, waits for them, and re-layouts  1.38 us (3%)
    pallas_call x1, Pallas kernels, local(): pl.pallas_call(kernel, out_shape=jax.ShapeDtypeStruct((128, 128), BF), in...  51.7 us
    unnamed x1, local copies, waits for them, and re-layouts  1.38 us

profile of v7, /device:TPU:1, one launch (start us, length us, event | category | flops | bytes accessed | tf_op | source)
XLA Modules:
  0.0 53.1 jit_solution(10426725412453619281)
XLA Ops:
  0.0 51.7 %shard_map.82 = bf16[128,128]{1,0:T(8,128)(2,1)} custom-call(bf16[128,128]{1,0:T(8,128)(2,1)} %tok_ref.1, f32[3,1024]{1,0:T(4,128)} %gain_ref.1, bf16[3,64,128]{2,1,0:T(8,128)(2,1)} %wq_ref.1, bf16[3,64,128]{2,1,0:T(8,128)(2,1)} %wk_ref.1, bf16[3,64,128]{2,1,0:T(8,128)(2,1)} %wv_ref.1, bf16[3,64,128]{2,1,0:T(8,128)(2,1)} %bitcast.3, f32[6,8,16]{2,1,0:T(8,128)} %bitcast.4, ...), custom_call_target="tpu_custom_call" | custom-call | tf_op jit(solution)/shard_map/pallas_call | solution.py:424
  51.7 1.4 %copy.10 = bf16[128,128]{1,0:T(8,128)(2,1)} copy(bf16[128,128]{1,0:T(8,128)(2,1)} %shard_map.82) | data formatting | bytes 65536

commit v8 on v7

--- a/solution.py
+++ b/solution.py
@@ -17,7 +17,7 @@
 RING = (2, 1, 3)
 TP_PEERS = ((2, 0), (2, 1), (1, 0), (3, 0), (1, 1), (3, 1), (0, 1))
 Y_FIRST = (32, 32)
-N_GROUPS = 64
+N_GROUPS = 51
 ALL_ROWS = 32768
 
 
@@ -108,7 +108,10 @@
             self.a, self.b = slice(low, mid), slice(mid, high)
             rows = slice(low, high)
             self.first = Group("p1_" + name, ref(0, slice(0, 3), rows))
-            self.second = Group("p2_" + name, ref(slice(0, 3), every, rows))
+            self.landing(name, rows)
+
+        def landing(self, name, rows):
+            self.second = Group("p2_" + name, self.ref(slice(0, 3), every, rows))
 
         def one(self):
             for d in RING:
@@ -129,11 +132,9 @@
             self.second.wait()
 
     class Relay(Plane):
-        def __init__(self, name, ref, low, high):
-            super().__init__(name, ref, low, high)
-            rows = slice(low, high)
-            self.near = Group("near_" + name, ref(slice(0, 2), every, rows))
-            self.far = Group("far_" + name, ref(0, every, rows))
+        def landing(self, name, rows):
+            self.near = Group("near_" + name, self.ref(slice(0, 2), every, rows))
+            self.far = Group("far_" + name, self.ref(0, every, rows))
 
         def two(self):
             self.first.wait()
@@ -373,8 +374,9 @@
         ) + BM[l]
         probs = jnp.exp(scores)
         norm = jnp.sum(probs, axis=1, keepdims=True)
-        mixed = jnp.dot(probs.astype(BF), KV[l, 1], preferred_element_type=F32) / norm
-        heads = jnp.where(left, mixed[:128], mixed[128:]).astype(BF)
+        mixed = jnp.dot(probs.astype(BF), KV[l, 1], preferred_element_type=F32)
+        heads = jnp.where(left, mixed[:128], mixed[128:]) / jnp.where(left, norm[:128], norm[128:])
+        heads = heads.astype(BF)
         if l < LAYERS - 1:
             A[l, y] = heads
             for d in RING:

time: 53.4 us -> 53.3 us (level)
  no operation moved by 1% of the time
where the time goes in v8:
time: 53.3 us; the launch traced here: 52.9 us
  Pallas kernels  51.6 us (97%)
  local copies, waits for them, and re-layouts  1.38 us (3%)
    pallas_call x1, Pallas kernels, local(): pl.pallas_call(kernel, out_shape=jax.ShapeDtypeStruct((128, 128), BF), in...  51.6 us
    unnamed x1, local copies, waits for them, and re-layouts  1.38 us

profile of v8, /device:TPU:1, one launch (start us, length us, event | category | flops | bytes accessed | tf_op | source)
XLA Modules:
  0.0 52.9 jit_solution(10444159042379482702)
XLA Ops:
  0.0 51.6 %shard_map.82 = bf16[128,128]{1,0:T(8,128)(2,1)} custom-call(bf16[128,128]{1,0:T(8,128)(2,1)} %tok_ref.1, f32[3,1024]{1,0:T(4,128)} %gain_ref.1, bf16[3,64,128]{2,1,0:T(8,128)(2,1)} %wq_ref.1, bf16[3,64,128]{2,1,0:T(8,128)(2,1)} %wk_ref.1, bf16[3,64,128]{2,1,0:T(8,128)(2,1)} %wv_ref.1, bf16[3,64,128]{2,1,0:T(8,128)(2,1)} %bitcast.3, f32[6,8,16]{2,1,0:T(8,128)} %bitcast.4, ...), custom_call_target="tpu_custom_call" | custom-call | tf_op jit(solution)/shard_map/pallas_call | solution.py:426
  51.6 1.4 %copy.10 = bf16[128,128]{1,0:T(8,128)(2,1)} copy(bf16[128,128]{1,0:T(8,128)(2,1)} %shard_map.82) | data formatting | bytes 65536
